TPU v7x, 32 devices: a whole 2x2x4 slice. The times are simulated.
32 devices in a mesh: sp: 8 (over z, y), tp: 4 (over x, core).
Axes of the slice: x: 2, y: 2, z: 4, core: 2. Of those that a mesh axis runs over, the one named last changes fastest.
Arguments:
- query_rows: bfloat16 [4096, 2048], P('sp', 'tp'), may hold values from -40 to 40
- key_rows: bfloat16 [4096, 256], P('sp', 'tp'), may hold values from -6 to 6
- value_rows: bfloat16 [4096, 256], P('sp', 'tp'), may hold values from -12 to 12
- doc_ids: int32 [4096], P('sp'), may hold values from 0 to 3, never falling along the last dimension, each value on 1 to 2048 neighbouring positions
- sink_logit: float32 [32], P('tp'), may hold values from 1 to 6
- residual: bfloat16 [4096, 2048], P('sp'), may hold values from -10 to 10
- out_proj: bfloat16 [2048, 2048], P('tp'), may hold values from -0.25 to 0.25
- mix_gain: float32 [2048], replicated, may hold values from 0.1 to 1.9
- gate_proj: bfloat16 [2048, 5632], P('sp', 'tp'), may hold values from -0.125 to 0.125
- value_proj: bfloat16 [2048, 5632], P('sp', 'tp'), may hold values from -0.125 to 0.125
- gate_taps: float32 [3, 5632], P(None, 'tp'), may hold values from -3 to 3
- value_taps: float32 [3, 5632], P(None, 'tp'), may hold values from -3 to 3
- down_proj: bfloat16 [5632, 2048], P('tp', 'sp'), may hold values from -0.078125 to 0.078125
- final_gain: float32 [2048], P('tp'), may hold values from 0.1 to 1.9
Outputs:
- mixed: bfloat16 [4096, 2048], P('sp', 'tp')
All inputs are finite; a program needn't handle non-finite values.
Results may differ from a plain program's by a relative error of at most 0.012.
Values may be sent and summed in bfloat16 or wider, within the bound.
A program may use at most 128 MiB of HBM per device.

v0:
```python
import functools
import math

import jax
import jax.numpy as jnp
from jax import lax
from jax.experimental import pallas as pl
from jax.experimental.pallas import tpu as pltpu
from jax.sharding import PartitionSpec as P

HD = 64
WIN = 128
TAPS = 3


mix_scale = math.sqrt(2.0)
norm_eps = 1e-05


def passed_along(block, axis, distance):
    devices = range(lax.axis_size(axis))
    route = [(i - distance, i) for i in devices if i - distance in devices]
    return lax.ppermute(block, axis, route)


def attend(query_block, key_block, value_block, query_pos, key_pos, query_doc, key_doc, sink):
    head_size = query_block.shape[-1]
    scores = jnp.einsum(
        "qkgd,skd->kgqs", query_block, key_block, preferred_element_type=jnp.float32
    ) * head_size ** (-0.5)
    diff = query_pos[:, None] - key_pos[None, :]
    valid = (
        (diff >= 0)
        & (diff < WIN)
        & (query_doc[:, None] == key_doc[None, :])
        & (key_pos[None, :] >= 0)
    )
    scores = jnp.where(valid[None, None], scores, -1e30)
    top = jnp.maximum(jnp.max(scores, axis=-1, keepdims=True), sink)
    weights = jnp.exp(scores - top)
    total = jnp.sum(weights, axis=-1, keepdims=True) + jnp.exp(sink - top)
    probs = (weights / total).astype(jnp.bfloat16)
    out = jnp.einsum("kgqs,skd->qkgd", probs, value_block, preferred_element_type=jnp.float32)
    return out.astype(jnp.bfloat16)


def depthwise(tail, current, taps, tail_docs, docs):
    extended = jnp.concatenate([tail, current])
    ext_docs = jnp.concatenate([tail_docs, docs])
    lag_rows = tail.shape[0]
    count = current.shape[0]
    total = jnp.zeros(current.shape, jnp.float32)
    for lag in range(lag_rows + 1):
        start = lag_rows - lag
        same = (ext_docs[start : start + count] == docs)[:, None]
        rows = extended[start : start + count].astype(jnp.float32)
        total = total + taps[lag][None, :] * jnp.where(same, rows, 0.0)
    return total


def on_device(
    query_rows,
    key_rows,
    value_rows,
    doc_ids,
    sink_logit,
    residual,
    out_proj,
    mix_gain,
    gate_proj,
    value_proj,
    gate_taps,
    value_taps,
    down_proj,
    final_gain,
):
    rows = query_rows.shape[0]
    kv_local = key_rows.shape[1] // HD
    heads_local = query_rows.shape[1] // HD
    groups = heads_local // kv_local
    offset = lax.axis_index("sp") * rows
    prev_keys, prev_values, prev_docs = passed_along(
        (key_rows[rows - WIN :], value_rows[rows - WIN :], doc_ids[rows - WIN :]), "sp", 1
    )
    all_keys = jnp.concatenate([prev_keys, key_rows]).reshape(rows + WIN, kv_local, HD)
    all_values = jnp.concatenate([prev_values, value_rows]).reshape(rows + WIN, kv_local, HD)
    all_docs = jnp.concatenate([prev_docs, doc_ids])
    key_pos = offset - WIN + jnp.arange(rows + WIN, dtype=jnp.int32)
    query_pos = offset + jnp.arange(rows, dtype=jnp.int32)
    queries = query_rows.reshape(rows, kv_local, groups, HD)
    sink = sink_logit.reshape(kv_local, groups, 1, 1)
    pieces = attend(queries, all_keys, all_values, query_pos, key_pos, doc_ids, all_docs, sink)
    heads = pieces.reshape(rows, heads_local * HD)
    partial_value = jnp.dot(heads, out_proj, preferred_element_type=jnp.float32)
    width = residual.shape[1]
    share = width // lax.axis_size("tp")
    col_start = lax.axis_index("tp") * share
    attn_total = lax.psum(partial_value.astype(jnp.bfloat16), "tp").astype(jnp.float32)
    first_sum = mix_scale * residual.astype(jnp.float32) + attn_total
    mean = jnp.mean(first_sum, axis=1, keepdims=True)
    var = jnp.mean(jnp.square(first_sum - mean), axis=1, keepdims=True)
    normed = ((first_sum - mean) * lax.rsqrt(var + norm_eps) * mix_gain[None, :]).astype(
        jnp.bfloat16
    )
    normed_own = lax.dynamic_slice_in_dim(normed, col_start, share, 1)
    up_gate = jnp.dot(
        normed,
        lax.all_gather(gate_proj, "sp", axis=0, tiled=True),
        preferred_element_type=jnp.float32,
    )
    up_value = jnp.dot(
        normed,
        lax.all_gather(value_proj, "sp", axis=0, tiled=True),
        preferred_element_type=jnp.float32,
    )
    up_gate = up_gate.astype(jnp.bfloat16)
    up_value = up_value.astype(jnp.bfloat16)
    lag_rows = TAPS - 1
    prev_gate, prev_value = passed_along(
        (up_gate[rows - lag_rows :], up_value[rows - lag_rows :]), "sp", 1
    )
    tail_docs = prev_docs[WIN - lag_rows :]
    conv_gate = depthwise(prev_gate, up_gate, gate_taps, tail_docs, doc_ids)
    conv_value = depthwise(prev_value, up_value, value_taps, tail_docs, doc_ids)
    hidden = (jax.nn.gelu(conv_gate) * conv_value).astype(jnp.bfloat16)
    terms = jnp.dot(
        hidden,
        lax.all_gather(down_proj, "sp", axis=1, tiled=True),
        preferred_element_type=jnp.float32,
    )
    ffn_own = lax.psum_scatter(
        terms.astype(jnp.bfloat16), "tp", scatter_dimension=1, tiled=True
    ).astype(jnp.float32)
    second_sum = mix_scale * normed_own.astype(jnp.float32) + ffn_own
    row_sum, row_squares = lax.psum(
        (jnp.sum(second_sum, axis=1), jnp.sum(second_sum * second_sum, axis=1)), "tp"
    )
    mean = row_sum / width
    var = row_squares / width - mean * mean
    return (
        (second_sum - mean[:, None]) * lax.rsqrt(var + norm_eps)[:, None] * final_gain[None, :]
    ).astype(jnp.bfloat16)


MESH = pl.DeviceIdType.MESH
LANES = 128
PAD = 16
F32 = jnp.float32
BF16 = jnp.bfloat16


def layer_kernel(
    n,
    n_tp,
    kv_ref,
    docs_ref,
    sink_ref,
    query_ref,
    out_proj_ref,
    residual_ref,
    mix_ref,
    gate_ref,
    value_ref,
    gate_taps_ref,
    value_taps_ref,
    down_ref,
    final_ref,
    out_ref,
    gate_all,
    value_all,
    down_all,
    kv_ext,
    docs_ext,
    docs_other,
    doc_cols,
    work_cols,
    taps_gate,
    taps_value,
    queries,
    proj,
    rest,
    heads,
    parts,
    parts_in,
    norm_own,
    norm_cols,
    normed,
    up_gate,
    up_value,
    hidden,
    terms,
    terms_in,
    second,
    stats,
    plane_send,
    row_send,
    core_send,
    block_recv,
    local_sem,
    taps_send,
    taps_recv,
    halo_send,
    halo_recv,
    rows_send,
    rows_recv,
    norm_send,
    norm_recv,
    cols_send,
    cols_recv,
    tail_send,
    tail_recv,
    term_send,
    term_recv,
    stat_send,
    stat_recv,
):
    sp = lax.axis_index("sp")
    tp = lax.axis_index("tp")
    rows = query_ref.shape[0]
    ff = gate_ref.shape[1]
    width = residual_ref.shape[1]
    depth = gate_ref.shape[0]
    cols = down_ref.shape[1]
    share = width // n_tp
    per = share // cols
    planes = n // 2
    z, y = sp // 2, lax.rem(sp, 2)
    x, core = tp // 2, lax.rem(tp, 2)
    low = lax.rem(z, 2)
    home = low == core
    base = sp - 2 * low
    work = base + 2 * core
    unit = 2 * x + low
    partner = base + 2 * (1 - low)
    sibling = 2 * x + 1 - core
    across = 2 * z + 1 - y
    after = lax.rem(sp + 1, n)
    peers = [lax.rem(tp + i, n_tp) for i in range(1, n_tp)]
    everyone = n * n_tp
    me = sp * n_tp + tp

    barrier = pltpu.get_barrier_semaphore()

    def greet(i, carry):
        other = lax.rem(me + i, everyone)
        pl.semaphore_signal(
            barrier,
            inc=1,
            device_id=(other // n_tp, lax.rem(other, n_tp)),
            device_id_type=MESH,
        )
        return carry

    lax.fori_loop(1, everyone, greet, 0)
    pl.semaphore_wait(barrier, everyone - 1)

    whole = (gate_all, value_all, down_all)
    own = (gate_ref, value_ref, down_ref)

    def slot(w, index):
        if w == 2:
            return down_all.at[index]
        return whole[w].at[pl.ds(pl.multiple_of(index * depth, depth), depth)]

    def to_plane(w, i):
        return pltpu.make_async_remote_copy(
            src_ref=own[w],
            dst_ref=slot(w, sp),
            send_sem=plane_send.at[w, i],
            recv_sem=block_recv.at[w, sp],
            device_id=(2 * (core + 2 * i) + y, tp),
            device_id_type=MESH,
        )

    def forward(w, index, source, sems, where, device):
        return pltpu.make_async_remote_copy(
            src_ref=source,
            dst_ref=slot(w, index),
            send_sem=sems.at[w, where],
            recv_sem=block_recv.at[w, index],
            device_id=device,
            device_id_type=MESH,
        )

    def to_row(w, at, source):
        return forward(w, 2 * at + y, source, row_send, at, (across, tp))

    def to_core(w, index, source):
        return forward(w, index, source, core_send, index, (sp, sibling))

    def await_block(w, index):
        to_core(w, index, slot(w, index)).wait_recv()

    def pass_own(w):
        to_row(w, z, own[w]).start()
        to_core(w, sp, own[w]).start()

    def service(kind, w, j):
        at = lax.rem(z + j, planes)

        @pl.when(home)
        def _():
            if kind == "own":
                pass_own(w)
            elif kind == "col":
                await_block(w, 2 * at + y)
                to_row(w, at, slot(w, 2 * at + y)).start()
                to_core(w, 2 * at + y, slot(w, 2 * at + y)).start()
            else:
                await_block(w, 2 * at + 1 - y)
                to_core(w, 2 * at + 1 - y, slot(w, 2 * at + 1 - y)).start()

    def plane_step(w):
        for i in range(planes // 2):
            @pl.when(core + 2 * i != z)
            def _():
                if w > 0:
                    to_plane(w - 1, i).wait_send()
                if w < 3:
                    to_plane(w, i).start()

    plane_step(0)
    service("own", 0, 0)
    service("own", 1, 0)

    halo = [
        pltpu.make_async_remote_copy(
            src_ref=kv_ref.at[pl.ds(rows - WIN, WIN)],
            dst_ref=kv_ext.at[pl.ds(0, WIN)],
            send_sem=halo_send.at[0],
            recv_sem=halo_recv.at[0],
            device_id=(after, tp),
            device_id_type=MESH,
        ),
        pltpu.make_async_remote_copy(
            src_ref=docs_ref.at[:, pl.ds(rows - WIN, WIN)],
            dst_ref=docs_ext.at[:, pl.ds(0, WIN)],
            send_sem=halo_send.at[1],
            recv_sem=halo_recv.at[1],
            device_id=(after, tp),
            device_id_type=MESH,
        ),
    ]
    for copy in halo:
        copy.start()
    row_share = rows // n_tp
    fetch = [
        pltpu.make_async_copy(kv_ref, kv_ext.at[pl.ds(WIN, rows)], local_sem.at[0]),
        pltpu.make_async_copy(docs_ref, docs_ext.at[:, pl.ds(WIN, rows)], local_sem.at[1]),
        pltpu.make_async_copy(query_ref, queries, local_sem.at[2]),
        pltpu.make_async_copy(out_proj_ref, proj, local_sem.at[3]),
        pltpu.make_async_copy(
            residual_ref.at[pl.ds(pl.multiple_of(tp * row_share, row_share), row_share)],
            rest,
            local_sem.at[4],
        ),
    ]
    for copy in fetch:
        copy.start()
    settle = [pltpu.make_async_copy(own[w], slot(w, sp), local_sem.at[5 + w]) for w in range(3)]
    settle.append(pltpu.make_async_copy(gate_taps_ref, taps_gate, local_sem.at[8]))
    settle.append(pltpu.make_async_copy(value_taps_ref, taps_value, local_sem.at[9]))
    taps = [
        pltpu.make_async_remote_copy(
            src_ref=source,
            dst_ref=target,
            send_sem=taps_send.at[i],
            recv_sem=taps_recv.at[i],
            device_id=(sp, sibling),
            device_id_type=MESH,
        )
        for i, (source, target) in enumerate(
            ((gate_taps_ref, taps_gate), (value_taps_ref, taps_value))
        )
    ]

    @pl.when(home)
    def _():
        for copy in settle + taps:
            copy.start()

    for copy in fetch:
        copy.wait()
    for copy in halo:
        copy.wait_recv()
    docs_copy = pltpu.make_async_remote_copy(
        src_ref=docs_ext,
        dst_ref=docs_other,
        send_sem=halo_send.at[2],
        recv_sem=halo_recv.at[2],
        device_id=(partner, tp),
        device_id_type=MESH,
    )
    docs_copy.start()

    line = lax.broadcasted_iota(jnp.int32, (LANES, LANES), 0)
    lane = lax.broadcasted_iota(jnp.int32, (LANES, LANES), 1)
    for b in range(rows // LANES + 1):
        row = docs_ext[0:1, b * LANES : (b + 1) * LANES].astype(F32)
        doc_cols[b * LANES : (b + 1) * LANES, :] = jnp.broadcast_to(row, (LANES, LANES)).T

    left = lax.broadcasted_iota(jnp.int32, (2 * WIN, LANES), 1) < HD
    zero = jnp.zeros((2 * WIN, LANES), BF16)

    def attend_block(b, carry):
        start = pl.multiple_of(b * WIN, WIN)
        kv = kv_ext[pl.ds(start, 2 * WIN), 0:LANES]
        vk = kv_ext[pl.ds(start, 2 * WIN), LANES : 2 * LANES]
        keys = jnp.concatenate([jnp.where(left, kv, zero), jnp.where(left, zero, vk)], axis=0)
        values = jnp.concatenate([jnp.where(left, vk, zero), jnp.where(left, zero, kv)], axis=0)
        query_doc = doc_cols[pl.ds(start + WIN, WIN), :]
        prev_doc = docs_ext[0:1, pl.ds(start, WIN)].astype(F32)
        this_doc = docs_ext[0:1, pl.ds(start + WIN, WIN)].astype(F32)
        prev_ok = (query_doc == prev_doc) & (lane > line) & (sp * rows + b * WIN > 0)
        this_ok = (query_doc == this_doc) & (lane <= line)
        bias = jnp.concatenate(
            [jnp.where(prev_ok, 0.0, -1e30), jnp.where(this_ok, 0.0, -1e30)], axis=1
        ).astype(F32)
        for pair in range(query_ref.shape[1] // LANES):
            block = queries[pl.ds(start, WIN), pair * LANES : (pair + 1) * LANES]
            both = lax.dot_general(
                block, keys, (((1,), (1,)), ((), ())), preferred_element_type=F32
            )
            probs = []
            for side in (0, 1):
                scores = both[:, side * 2 * WIN : (side + 1) * 2 * WIN] * HD ** (-0.5) + bias
                sink = sink_ref[2 * pair + side]
                top = jnp.maximum(jnp.max(scores, axis=1, keepdims=True), sink)
                weights = jnp.exp(scores - top)
                total = jnp.sum(weights, axis=1, keepdims=True) + jnp.exp(sink - top)
                probs.append((weights / total).astype(BF16))
            heads[:, pair * LANES : (pair + 1) * LANES] = jnp.dot(
                jnp.concatenate(probs, axis=1), values, preferred_element_type=F32
            ).astype(BF16)
        for c in range(width // 512):
            parts[b, :, c * 512 : (c + 1) * 512] = jnp.dot(
                heads[...], proj[:, c * 512 : (c + 1) * 512], preferred_element_type=F32
            ).astype(BF16)

        @pl.when(b == n_tp - 1)
        def _():
            plane_step(1)

        for j in range(1, planes):
            @pl.when(b == min(j, n_tp - 1))
            def _():
                service("col", 0, j)

        return carry

    lax.fori_loop(0, n_tp, attend_block, 0)

    def rows_copy(peer, source):
        return pltpu.make_async_remote_copy(
            src_ref=parts.at[peer],
            dst_ref=parts_in.at[source],
            send_sem=rows_send.at[peer],
            recv_sem=rows_recv.at[source],
            device_id=(sp, peer),
            device_id_type=MESH,
        )

    for peer in peers:
        rows_copy(peer, tp).start()
    for peer in peers:
        rows_copy(peer, peer).wait_recv()
    first = mix_scale * rest[...].astype(F32) + parts[tp].astype(F32)
    for peer in peers:
        first = first + parts_in[peer].astype(F32)
    mean = jnp.mean(first, axis=1, keepdims=True)
    first = first - mean
    var = jnp.mean(first * first, axis=1, keepdims=True)
    norm_own[...] = (first * lax.rsqrt(var + norm_eps) * mix_ref[...]).astype(BF16)

    def workers(block):
        parity = lax.rem(block // 2, 2)
        return [
            (block - 2 * parity + 2 * a, 2 * b + parity)
            for a in (0, 1)
            for b in range(n_tp // 2)
        ]

    def place_of(source):
        return pl.ds(pl.multiple_of(PAD + source * row_share, PAD), row_share)

    def norm_copy(i, device, source):
        return pltpu.make_async_remote_copy(
            src_ref=norm_own,
            dst_ref=normed.at[place_of(source)],
            send_sem=norm_send.at[i],
            recv_sem=norm_recv.at[source],
            device_id=device,
            device_id_type=MESH,
        )

    def is_me(device):
        return (device[0] == sp) & (device[1] == tp)

    def cols_copy(i, peer, source):
        rows_at = pl.ds(pl.multiple_of(source * row_share, row_share), row_share)
        return pltpu.make_async_remote_copy(
            src_ref=norm_own.at[:, pl.ds(pl.multiple_of(peer * share, share), share)],
            dst_ref=norm_cols.at[rows_at],
            send_sem=cols_send.at[i],
            recv_sem=cols_recv.at[source],
            device_id=(sp, peer),
            device_id_type=MESH,
        )

    def tail_copy(i, device):
        return pltpu.make_async_remote_copy(
            src_ref=norm_own.at[pl.ds(row_share - PAD, PAD)],
            dst_ref=normed.at[pl.ds(0, PAD)],
            send_sem=tail_send.at[i],
            recv_sem=tail_recv,
            device_id=device,
            device_id_type=MESH,
        )

    own_workers = workers(sp)
    next_workers = workers(after)
    for i, device in enumerate(own_workers):
        @pl.when(jnp.logical_not(is_me(device)))
        def _():
            norm_copy(i, device, tp).start()

    @pl.when(tp == n_tp - 1)
    def _():
        for i, device in enumerate(next_workers):
            tail_copy(i, device).start()

    for i, peer in enumerate(peers):
        cols_copy(i, peer, tp).start()
    service("col", 1, 1)
    plane_step(2)

    @pl.when(home)
    def _():
        normed[place_of(tp), :] = norm_own[...]

    norm_cols[pl.ds(pl.multiple_of(tp * row_share, row_share), row_share), :] = norm_own[
        :, pl.ds(pl.multiple_of(tp * share, share), share)
    ]
    for j in range(planes):
        service("row", 0, j)
    for j in range(2, planes):
        service("col", 1, j)
    service("own", 2, 0)
    for j in range(planes):
        service("row", 1, j)
    docs_copy.wait_recv()
    for b in range(rows // LANES + 1):
        part = slice(b * LANES, (b + 1) * LANES)
        row = jnp.where(home, docs_ext[0:1, part], docs_other[0:1, part]).astype(F32)
        work_cols[part, :] = jnp.broadcast_to(row, (LANES, LANES)).T

    for source in range(n_tp):
        @pl.when(jnp.logical_not(home & (tp == source)))
        def _():
            norm_copy(0, (sp, sibling), source).wait_recv()

    tail_copy(0, (sp, sibling)).wait_recv()

    @pl.when(home)
    def _():
        for copy in settle:
            copy.wait()

    @pl.when(jnp.logical_not(home))
    def _():
        for copy in taps:
            copy.wait_recv()
        for w in (0, 1):
            for index in range(n):
                await_block(w, index)

    place = lax.broadcasted_iota(jnp.int32, (rows, LANES), 0) + work * rows

    def convolved(source, taps_ref, at):
        total = taps_ref[0:1, pl.ds(at, LANES)] * source[PAD : PAD + rows, :]
        doc = work_cols[WIN : WIN + rows, :]
        for lag in range(1, TAPS):
            same = (work_cols[WIN - lag : WIN - lag + rows, :] == doc) & (place >= lag)
            shifted = jnp.where(same, source[PAD - lag : PAD - lag + rows, :], 0.0)
            total = total + taps_ref[lag : lag + 1, pl.ds(at, LANES)] * shifted
        return total

    def up_block(c, carry):
        at = pl.multiple_of(c * LANES, LANES)
        weights = jnp.concatenate(
            [gate_all[:, pl.ds(at, LANES)], value_all[:, pl.ds(at, LANES)]], axis=1
        )
        both = jnp.dot(normed[...], weights, preferred_element_type=F32)
        both = both.astype(BF16).astype(F32)
        up_gate[...] = both[:, :LANES]
        up_value[...] = both[:, LANES:]
        gate = convolved(up_gate, taps_gate, at)
        value = convolved(up_value, taps_value, at)
        inner = math.sqrt(2.0 / math.pi) * (gate + 0.044715 * (gate * gate * gate))
        hidden[:, pl.ds(at, LANES)] = (0.5 * gate * (1.0 + jnp.tanh(inner)) * value).astype(BF16)
        for j in range(1, planes):
            @pl.when(c == 3 * j - 2)
            def _():
                service("col", 2, j)

        for j in (0, 1):
            @pl.when(c == 6 + 2 * j)
            def _():
                service("row", 2, j)

        return carry

    lax.fori_loop(0, ff // LANES, up_block, 0)
    for j in range(2, planes):
        service("row", 2, j)

    @pl.when(jnp.logical_not(home))
    def _():
        for index in range(n):
            await_block(2, index)

    def term_copy(index, source):
        owner = index // per
        return pltpu.make_async_remote_copy(
            src_ref=terms.at[index],
            dst_ref=terms_in.at[source, lax.rem(index, per)],
            send_sem=term_send.at[index],
            recv_sem=term_recv.at[source, lax.rem(index, per)],
            device_id=(work, owner),
            device_id_type=MESH,
        )

    def down_block(q, carry):
        index = lax.rem(q + per * 2 * (1 - x), n)
        terms[index] = jnp.dot(
            hidden[...], down_all[index], preferred_element_type=F32
        ).astype(BF16)

        mine = home & (index // per == tp)

        @pl.when(mine)
        def _():
            terms_in[tp, lax.rem(index, per)] = terms[index]

        @pl.when(jnp.logical_not(mine))
        def _():
            term_copy(index, unit).start()

        return carry

    lax.fori_loop(0, n, down_block, 0)

    for source in range(n_tp):
        @pl.when(jnp.logical_not(home & (tp == source)))
        def _():
            for j in range(per):
                pltpu.make_async_remote_copy(
                    src_ref=terms_in.at[source, j],
                    dst_ref=terms_in.at[source, j],
                    send_sem=term_send.at[0],
                    recv_sem=term_recv.at[source, j],
                    device_id=(sp, sibling),
                    device_id_type=MESH,
                ).wait_recv()

    for i, peer in enumerate(peers):
        cols_copy(i, peer, peer).wait_recv()

    sums = jnp.zeros((rows, 1), F32)
    squares = jnp.zeros((rows, 1), F32)
    for j in range(per):
        total = mix_scale * norm_cols[:, j * cols : (j + 1) * cols].astype(F32)
        for source in range(n_tp):
            total = total + terms_in[source, j].astype(F32)
        second[:, j * cols : (j + 1) * cols] = total
        sums = sums + jnp.sum(total, axis=1, keepdims=True)
        squares = squares + jnp.sum(total * total, axis=1, keepdims=True)
    which = lax.broadcasted_iota(jnp.int32, (rows, LANES), 1)
    packed = jnp.where(which == 0, sums, jnp.where(which == 1, squares, 0.0))
    stats[tp] = packed.T[0:8]

    def stat_copy(peer, source):
        return pltpu.make_async_remote_copy(
            src_ref=stats.at[source],
            dst_ref=stats.at[source],
            send_sem=stat_send.at[peer],
            recv_sem=stat_recv.at[source],
            device_id=(sp, peer),
            device_id_type=MESH,
        )

    for peer in peers:
        stat_copy(peer, tp).start()
    for peer in peers:
        stat_copy(peer, peer).wait_recv()
    total = stats[0]
    for source in range(1, n_tp):
        total = total + stats[source]
    spread = jnp.concatenate([total] * (LANES // 8), axis=0).T
    mean = spread[:, 0:1] / width
    var = spread[:, 1:2] / width - mean * mean
    out_ref[...] = (
        (second[...] - mean) * lax.rsqrt(var + norm_eps) * final_ref[...]
    ).astype(BF16)

    plane_step(3)

    @pl.when(home)
    def _():
        for w in range(3):
            for at in range(planes):
                to_row(w, at, slot(w, sp)).wait_send()
            for index in range(n):
                to_core(w, index, slot(w, index)).wait_send()
        for copy in taps:
            copy.wait_send()

    for copy in halo:
        copy.wait_send()
    docs_copy.wait_send()
    for i, device in enumerate(own_workers):
        @pl.when(jnp.logical_not(is_me(device)))
        def _():
            norm_copy(i, device, tp).wait_send()

    @pl.when(tp == n_tp - 1)
    def _():
        for i, device in enumerate(next_workers):
            tail_copy(i, device).wait_send()

    for i, peer in enumerate(peers):
        rows_copy(peer, tp).wait_send()
        cols_copy(i, peer, tp).wait_send()
        stat_copy(peer, tp).wait_send()
    for index in range(n):
        @pl.when(jnp.logical_not(home & (tp == index // per)))
        def _():
            term_copy(index, unit).wait_send()


def fused(
    query_rows,
    key_rows,
    value_rows,
    doc_ids,
    sink_logit,
    residual,
    out_proj,
    mix_gain,
    gate_proj,
    value_proj,
    gate_taps,
    value_taps,
    down_proj,
    final_gain,
):
    n = lax.axis_size("sp")
    n_tp = lax.axis_size("tp")
    rows, head_cols = query_rows.shape
    width = residual.shape[1]
    depth, ff = gate_proj.shape
    cols = down_proj.shape[1]
    per = width // n_tp // cols
    planes = n // 2
    kv = jnp.concatenate([key_rows, value_rows, value_rows, key_rows], axis=1)
    docs = jnp.broadcast_to(doc_ids[None, :], (8, rows))
    share = rows // n_tp
    anywhere = pl.BlockSpec(memory_space=pl.ANY)
    vmem = pl.BlockSpec(memory_space=pltpu.VMEM)
    smem = pl.BlockSpec(memory_space=pltpu.SMEM)
    dma = pltpu.SemaphoreType.DMA
    return pl.pallas_call(
        functools.partial(layer_kernel, n, n_tp),
        out_shape=jax.ShapeDtypeStruct((rows, width // n_tp), BF16),
        in_specs=[
            anywhere, anywhere, smem, anywhere, anywhere, anywhere, vmem,
            anywhere, anywhere, anywhere, anywhere, anywhere, vmem,
        ],
        out_specs=vmem,
        scratch_shapes=[
            pltpu.VMEM((n * depth, ff), BF16),
            pltpu.VMEM((n * depth, ff), BF16),
            pltpu.VMEM((n, ff, cols), BF16),
            pltpu.VMEM((WIN + rows, 4 * HD), BF16),
            pltpu.VMEM((8, WIN + rows), jnp.int32),
            pltpu.VMEM((8, WIN + rows), jnp.int32),
            pltpu.VMEM((WIN + rows, LANES), F32),
            pltpu.VMEM((WIN + rows, LANES), F32),
            pltpu.VMEM(gate_taps.shape, F32),
            pltpu.VMEM(gate_taps.shape, F32),
            pltpu.VMEM((rows, head_cols), BF16),
            pltpu.VMEM((head_cols, width), BF16),
            pltpu.VMEM((share, width), BF16),
            pltpu.VMEM((share, head_cols), BF16),
            pltpu.VMEM((n_tp, share, width), BF16),
            pltpu.VMEM((n_tp, share, width), BF16),
            pltpu.VMEM((share, width), BF16),
            pltpu.VMEM((rows, width // n_tp), BF16),
            pltpu.VMEM((PAD + rows, width), BF16),
            pltpu.VMEM((PAD + rows, LANES), F32),
            pltpu.VMEM((PAD + rows, LANES), F32),
            pltpu.VMEM((rows, ff), BF16),
            pltpu.VMEM((n, rows, cols), BF16),
            pltpu.VMEM((n_tp, per, rows, cols), BF16),
            pltpu.VMEM((rows, width // n_tp), F32),
            pltpu.VMEM((n_tp, 8, rows), F32),
            dma((3, planes // 2)),
            dma((3, planes)),
            dma((3, n)),
            dma((3, n)),
            dma((10,)),
            dma((2,)),
            dma((2,)),
            dma((3,)),
            dma((3,)),
            dma((n_tp,)),
            dma((n_tp,)),
            dma((n_tp,)),
            dma((n_tp,)),
            dma((n_tp,)),
            dma((n_tp,)),
            dma((n_tp,)),
            dma(()),
            dma((n,)),
            dma((n_tp, per)),
            dma((n_tp,)),
            dma((n_tp,)),
        ],
        compiler_params=pltpu.CompilerParams(
            collective_id=0, has_side_effects=True, vmem_limit_bytes=60 * 1024 * 1024
        ),
        name="layer",
    )(
        kv,
        docs,
        sink_logit,
        query_rows,
        out_proj,
        residual,
        mix_gain[None, :],
        gate_proj,
        value_proj,
        gate_taps,
        value_taps,
        down_proj,
        final_gain[None, :],
    )


def on_any(*args):
    query_rows, key_rows, gate_proj, down_proj = args[0], args[1], args[8], args[12]
    n, n_tp = lax.axis_size("sp"), lax.axis_size("tp")
    share = args[5].shape[1] // n_tp
    depth, ff = gate_proj.shape
    cols = down_proj.shape[1]
    fits = (
        n % 4 == 0
        and n_tp == 4
        and n >= 8
        and n <= n_tp * 2
        and ff >= 10 * LANES
        and query_rows.shape[0] == n_tp * WIN
        and key_rows.shape[1] == HD
        and query_rows.shape[1] % LANES == 0
        and depth % 32 == 0
        and ff % LANES == 0
        and cols % LANES == 0
        and share % cols == 0
    )
    return fused(*args) if fits else on_device(*args)


def solution(mesh):
    placed = (
        P("sp", "tp"),
        P("sp", "tp"),
        P("sp", "tp"),
        P("sp"),
        P("tp"),
        P("sp", None),
        P("tp", None),
        P(),
        P("sp", "tp"),
        P("sp", "tp"),
        P(None, "tp"),
        P(None, "tp"),
        P("tp", "sp"),
        P("tp"),
    )
    return jax.shard_map(
        on_any, mesh=mesh, in_specs=placed, out_specs=P("sp", "tp"), check_vma=False
    )
```

profile of v0, /device:TPU:0, one launch (start us, length us, event | category | flops | bytes accessed | tf_op | source)
XLA Modules:
  0.0 177.0 jit_solution(13203863922392797569)
XLA Ops:
  0.0 1.3 broadcast_in_dim.12.docs_ref
  1.3 1.0 copy.15
  2.2 1.0 copy.16
  3.2 0.9 pad_maximum_fusion.kv_ref
  4.1 171.0 %layer.1 = bf16[512,512]{1,0:T(8,128)(2,1)} custom-call(bf16[512,256]{1,0:T(8,128)(2,1)} %pad_maximum_fusion.kv_ref, s32[8,512]{1,0:T(8,128)} %broadcast_in_dim.12.docs_ref, f32[8]{0:T(128)} %sink_ref.1, bf16[512,512]{1,0:T(8,128)(2,1)} %query_ref.1, bf16[512,2048]{1,0:T(8,128)(2,1)} %out_proj_ref.1, bf16[512,2048]{1,0:T(8,128)(2,1)} %residual_ref.1, ...), custom_call_target="tpu_custom_call" | custom-call | tf_op jit(solution)/shard_map/layer/pallas_call | solution.py:772
  175.1 1.9 %copy.20 = bf16[512,512]{1,0:T(8,128)(2,1)} copy(bf16[512,512]{1,0:T(8,128)(2,1)} %layer.1) | data formatting | bytes 1048576
where the time goes:
time: 180 us; the launch traced here: 177 us
  Pallas kernels  171 us (95%)
  local copies, waits for them, and re-layouts  5.06 us (3%)
    pallas_call x1, Pallas kernels, fused(): pl.pallas_call(functools.partial(layer_kernel, n, n_tp), out_shape=jax.Sh...  171 us
    unnamed x3, local copies, waits for them, and re-layouts  3.78 us

commit v1 on v0

--- a/solution.py
+++ b/solution.py
@@ -145,6 +145,7 @@
 MESH = pl.DeviceIdType.MESH
 LANES = 128
 PAD = 16
+CHUNKS = 4
 F32 = jnp.float32
 BF16 = jnp.bfloat16
 
@@ -152,8 +153,9 @@
 def layer_kernel(
     n,
     n_tp,
-    kv_ref,
-    docs_ref,
+    key_ref,
+    val_ref,
+    aux_ref,
     sink_ref,
     query_ref,
     out_proj_ref,
@@ -161,21 +163,19 @@
     mix_ref,
     gate_ref,
     value_ref,
-    gate_taps_ref,
-    value_taps_ref,
     down_ref,
     final_ref,
     out_ref,
     gate_all,
     value_all,
     down_all,
-    kv_ext,
+    key_ext,
+    val_ext,
     docs_ext,
     docs_other,
     doc_cols,
-    work_cols,
-    taps_gate,
-    taps_value,
+    mask_cols,
+    taps_all,
     queries,
     proj,
     rest,
@@ -196,6 +196,7 @@
     row_send,
     core_send,
     block_recv,
+    core_recv,
     local_sem,
     taps_send,
     taps_recv,
@@ -227,17 +228,21 @@
     z, y = sp // 2, lax.rem(sp, 2)
     x, core = tp // 2, lax.rem(tp, 2)
     low = lax.rem(z, 2)
+    half = z // 2
+    inner = lax.rem(low + half, 2) == 1
     home = low == core
     base = sp - 2 * low
     work = base + 2 * core
     unit = 2 * x + low
     partner = base + 2 * (1 - low)
     sibling = 2 * x + 1 - core
+    facing = 2 * (1 - x) + core
     across = 2 * z + 1 - y
     after = lax.rem(sp + 1, n)
     peers = [lax.rem(tp + i, n_tp) for i in range(1, n_tp)]
     everyone = n * n_tp
     me = sp * n_tp + tp
+    row_share = rows // n_tp
 
     barrier = pltpu.get_barrier_semaphore()
 
@@ -252,165 +257,227 @@
         return carry
 
     lax.fori_loop(1, everyone, greet, 0)
-    pl.semaphore_wait(barrier, everyone - 1)
-
-    whole = (gate_all, value_all, down_all)
-    own = (gate_ref, value_ref, down_ref)
-
-    def slot(w, index):
-        if w == 2:
-            return down_all.at[index]
-        return whole[w].at[pl.ds(pl.multiple_of(index * depth, depth), depth)]
-
-    def to_plane(w, i):
-        return pltpu.make_async_remote_copy(
-            src_ref=own[w],
-            dst_ref=slot(w, sp),
-            send_sem=plane_send.at[w, i],
-            recv_sem=block_recv.at[w, sp],
-            device_id=(2 * (core + 2 * i) + y, tp),
-            device_id_type=MESH,
-        )
-
-    def forward(w, index, source, sems, where, device):
-        return pltpu.make_async_remote_copy(
-            src_ref=source,
-            dst_ref=slot(w, index),
-            send_sem=sems.at[w, where],
-            recv_sem=block_recv.at[w, index],
-            device_id=device,
-            device_id_type=MESH,
-        )
-
-    def to_row(w, at, source):
-        return forward(w, 2 * at + y, source, row_send, at, (across, tp))
-
-    def to_core(w, index, source):
-        return forward(w, index, source, core_send, index, (sp, sibling))
-
-    def await_block(w, index):
-        to_core(w, index, slot(w, index)).wait_recv()
-
-    def pass_own(w):
-        to_row(w, z, own[w]).start()
-        to_core(w, sp, own[w]).start()
-
-    def service(kind, w, j):
-        at = lax.rem(z + j, planes)
-
-        @pl.when(home)
-        def _():
-            if kind == "own":
-                pass_own(w)
-            elif kind == "col":
-                await_block(w, 2 * at + y)
-                to_row(w, at, slot(w, 2 * at + y)).start()
-                to_core(w, 2 * at + y, slot(w, 2 * at + y)).start()
-            else:
-                await_block(w, 2 * at + 1 - y)
-                to_core(w, 2 * at + 1 - y, slot(w, 2 * at + 1 - y)).start()
-
-    def plane_step(w):
-        for i in range(planes // 2):
-            @pl.when(core + 2 * i != z)
-            def _():
-                if w > 0:
-                    to_plane(w - 1, i).wait_send()
-                if w < 3:
-                    to_plane(w, i).start()
-
-    plane_step(0)
-    service("own", 0, 0)
-    service("own", 1, 0)
-
-    halo = [
-        pltpu.make_async_remote_copy(
-            src_ref=kv_ref.at[pl.ds(rows - WIN, WIN)],
-            dst_ref=kv_ext.at[pl.ds(0, WIN)],
-            send_sem=halo_send.at[0],
-            recv_sem=halo_recv.at[0],
-            device_id=(after, tp),
-            device_id_type=MESH,
-        ),
-        pltpu.make_async_remote_copy(
-            src_ref=docs_ref.at[:, pl.ds(rows - WIN, WIN)],
-            dst_ref=docs_ext.at[:, pl.ds(0, WIN)],
-            send_sem=halo_send.at[1],
-            recv_sem=halo_recv.at[1],
-            device_id=(after, tp),
-            device_id_type=MESH,
-        ),
-    ]
-    for copy in halo:
-        copy.start()
-    row_share = rows // n_tp
+    docs_ref = aux_ref.at[:, pl.ds(ff, rows)]
     fetch = [
-        pltpu.make_async_copy(kv_ref, kv_ext.at[pl.ds(WIN, rows)], local_sem.at[0]),
-        pltpu.make_async_copy(docs_ref, docs_ext.at[:, pl.ds(WIN, rows)], local_sem.at[1]),
-        pltpu.make_async_copy(query_ref, queries, local_sem.at[2]),
-        pltpu.make_async_copy(out_proj_ref, proj, local_sem.at[3]),
+        pltpu.make_async_copy(key_ref, key_ext.at[pl.ds(WIN, rows)], local_sem.at[0]),
+        pltpu.make_async_copy(val_ref, val_ext.at[pl.ds(WIN, rows)], local_sem.at[1]),
+        pltpu.make_async_copy(docs_ref, docs_ext.at[:, pl.ds(WIN, rows)], local_sem.at[2]),
+        pltpu.make_async_copy(query_ref, queries, local_sem.at[3]),
+        pltpu.make_async_copy(out_proj_ref, proj, local_sem.at[4]),
         pltpu.make_async_copy(
             residual_ref.at[pl.ds(pl.multiple_of(tp * row_share, row_share), row_share)],
             rest,
-            local_sem.at[4],
+            local_sem.at[5],
         ),
     ]
     for copy in fetch:
         copy.start()
-    settle = [pltpu.make_async_copy(own[w], slot(w, sp), local_sem.at[5 + w]) for w in range(3)]
-    settle.append(pltpu.make_async_copy(gate_taps_ref, taps_gate, local_sem.at[8]))
-    settle.append(pltpu.make_async_copy(value_taps_ref, taps_value, local_sem.at[9]))
-    taps = [
+    pl.semaphore_wait(barrier, everyone - 1)
+
+    whole = (gate_all, value_all, down_all)
+    own = (gate_ref, value_ref, down_ref)
+    sizes = (depth // CHUNKS, depth // CHUNKS, ff // CHUNKS)
+
+    def piece(w, q):
+        return own[w].at[pl.ds(q * sizes[w], sizes[w])]
+
+    def slot(w, index, q):
+        if w == 2:
+            return down_all.at[index, pl.ds(q * sizes[2], sizes[2])]
+        return whole[w].at[
+            pl.ds(pl.multiple_of(index * depth + q * sizes[w], sizes[w]), sizes[w])
+        ]
+
+    def slab(w, index):
+        if w == 2:
+            return down_all.at[index]
+        return whole[w].at[pl.ds(pl.multiple_of(index * depth, depth), depth)]
+
+    def to_plane(w, i, q):
+        return pltpu.make_async_remote_copy(
+            src_ref=piece(w, q),
+            dst_ref=slot(w, sp, q),
+            send_sem=plane_send.at[w, i, q],
+            recv_sem=block_recv.at[w, sp, q],
+            device_id=(2 * (core + 2 * i) + y, tp),
+            device_id_type=MESH,
+        )
+
+    def to_row(w, at, q, source):
+        return pltpu.make_async_remote_copy(
+            src_ref=source,
+            dst_ref=slot(w, 2 * at + y, q),
+            send_sem=row_send.at[w, at, q],
+            recv_sem=block_recv.at[w, 2 * at + y, q],
+            device_id=(across, tp),
+            device_id_type=MESH,
+        )
+
+    def to_core(w, index, q, source):
+        return pltpu.make_async_remote_copy(
+            src_ref=source,
+            dst_ref=slot(w, index, q),
+            send_sem=core_send.at[w, index, q],
+            recv_sem=core_recv.at[w, index, q],
+            device_id=(sp, sibling),
+            device_id_type=MESH,
+        )
+
+    def await_piece(w, index, q):
+        pltpu.make_async_remote_copy(
+            src_ref=slot(w, index, q),
+            dst_ref=slot(w, index, q),
+            send_sem=core_send.at[w, index, q],
+            recv_sem=block_recv.at[w, index, q],
+            device_id=(sp, sibling),
+            device_id_type=MESH,
+        ).wait_recv()
+
+    def near_sends(w):
+        for i in range(2):
+            @pl.when((half == i) & (core + 2 * i != z))
+            def _():
+                for q in range(CHUNKS):
+                    to_plane(w, i, q).start()
+
+    def far_sends(w, cond):
+        for i in range(2):
+            @pl.when((half != i) & cond)
+            def _():
+                for q in range(CHUNKS):
+                    to_plane(w, i, q).start()
+
+    def zone(k):
+        block = lax.rem(half + k // 2, 2)
+        side = low if k < 2 else half
+        return 2 * block + lax.rem(side + k % 2, 2)
+
+    def own_row(w):
+        @pl.when(home)
+        def _():
+            for q in range(CHUNKS):
+                to_row(w, z, q, piece(w, q)).start()
+
+    def own_core(w):
+        @pl.when(home)
+        def _():
+            for q in range(CHUNKS):
+                to_core(w, sp, q, piece(w, q)).start()
+
+    def col(w, k, q):
+        at = zone(k)
+        index = 2 * at + y
+        await_piece(w, index, q)
+        to_row(w, at, q, slot(w, index, q)).start()
+        to_core(w, index, q, slot(w, index, q)).start()
+
+    def row(w, k, q):
+        index = 2 * zone(k) + 1 - y
+        await_piece(w, index, q)
+        to_core(w, index, q, slot(w, index, q)).start()
+
+    halo = [
         pltpu.make_async_remote_copy(
             src_ref=source,
             dst_ref=target,
-            send_sem=taps_send.at[i],
-            recv_sem=taps_recv.at[i],
-            device_id=(sp, sibling),
+            send_sem=halo_send.at[i],
+            recv_sem=halo_recv.at[i],
+            device_id=(after, tp),
             device_id_type=MESH,
         )
         for i, (source, target) in enumerate(
-            ((gate_taps_ref, taps_gate), (value_taps_ref, taps_value))
+            (
+                (key_ref.at[pl.ds(rows - WIN, WIN)], key_ext.at[pl.ds(0, WIN)]),
+                (val_ref.at[pl.ds(rows - WIN, WIN)], val_ext.at[pl.ds(0, WIN)]),
+                (
+                    aux_ref.at[:, pl.ds(ff + rows - WIN, WIN)],
+                    docs_ext.at[:, pl.ds(0, WIN)],
+                ),
+            )
         )
     ]
+    for copy in halo:
+        copy.start()
+    near_sends(0)
+    far_sends(0, True)
+    own_row(0)
+    own_row(1)
+    near_sends(1)
+    far_sends(1, inner)
+    settle = [
+        pltpu.make_async_copy(own[w], slab(w, sp), local_sem.at[6 + w]) for w in range(3)
+    ]
+    settle.append(
+        pltpu.make_async_copy(aux_ref.at[:, pl.ds(0, ff)], taps_all, local_sem.at[9])
+    )
+    taps_copy = pltpu.make_async_remote_copy(
+        src_ref=aux_ref.at[:, pl.ds(0, ff)],
+        dst_ref=taps_all,
+        send_sem=taps_send,
+        recv_sem=taps_recv,
+        device_id=(sp, sibling),
+        device_id_type=MESH,
+    )
 
     @pl.when(home)
     def _():
-        for copy in settle + taps:
+        for copy in settle:
             copy.start()
-
+        taps_copy.start()
+
+    own_core(0)
+    own_core(1)
     for copy in fetch:
         copy.wait()
-    for copy in halo:
-        copy.wait_recv()
-    docs_copy = pltpu.make_async_remote_copy(
-        src_ref=docs_ext,
-        dst_ref=docs_other,
-        send_sem=halo_send.at[2],
-        recv_sem=halo_recv.at[2],
-        device_id=(partner, tp),
-        device_id_type=MESH,
-    )
-    docs_copy.start()
 
     line = lax.broadcasted_iota(jnp.int32, (LANES, LANES), 0)
     lane = lax.broadcasted_iota(jnp.int32, (LANES, LANES), 1)
-    for b in range(rows // LANES + 1):
-        row = docs_ext[0:1, b * LANES : (b + 1) * LANES].astype(F32)
-        doc_cols[b * LANES : (b + 1) * LANES, :] = jnp.broadcast_to(row, (LANES, LANES)).T
-
-    left = lax.broadcasted_iota(jnp.int32, (2 * WIN, LANES), 1) < HD
-    zero = jnp.zeros((2 * WIN, LANES), BF16)
-
-    def attend_block(b, carry):
+    for b in range(1, rows // LANES + 1):
+        row_doc = docs_ext[0:1, b * LANES : (b + 1) * LANES]
+        doc_cols[b * LANES : (b + 1) * LANES, :] = jnp.broadcast_to(row_doc, (LANES, LANES)).T
+
+    zero = jnp.zeros((2 * WIN, HD), BF16)
+
+    def pair_copy(i, block):
+        return pltpu.make_async_remote_copy(
+            src_ref=parts.at[block],
+            dst_ref=parts_in.at[i],
+            send_sem=rows_send.at[i],
+            recv_sem=rows_recv.at[i],
+            device_id=(sp, sibling),
+            device_id_type=MESH,
+        )
+
+    def facing_copy():
+        return pltpu.make_async_remote_copy(
+            src_ref=parts.at[facing],
+            dst_ref=parts_in.at[2],
+            send_sem=rows_send.at[2],
+            recv_sem=rows_recv.at[2],
+            device_id=(sp, facing),
+            device_id_type=MESH,
+        )
+
+    def attend_block(j, carry):
+        b = 2 * lax.rem(x + 1 + j, 2) + lax.rem(core + 1 + j // 2, 2)
+
+        @pl.when(b == 0)
+        def _():
+            for copy in halo:
+                copy.wait_recv()
+
         start = pl.multiple_of(b * WIN, WIN)
-        kv = kv_ext[pl.ds(start, 2 * WIN), 0:LANES]
-        vk = kv_ext[pl.ds(start, 2 * WIN), LANES : 2 * LANES]
-        keys = jnp.concatenate([jnp.where(left, kv, zero), jnp.where(left, zero, vk)], axis=0)
-        values = jnp.concatenate([jnp.where(left, vk, zero), jnp.where(left, zero, kv)], axis=0)
+        k = key_ext[pl.ds(start, 2 * WIN), :]
+        v = val_ext[pl.ds(start, 2 * WIN), :]
+        keys = jnp.concatenate(
+            [jnp.concatenate([k, zero], axis=1), jnp.concatenate([zero, k], axis=1)], axis=0
+        )
+        values = jnp.concatenate(
+            [jnp.concatenate([v, zero], axis=1), jnp.concatenate([zero, v], axis=1)], axis=0
+        )
         query_doc = doc_cols[pl.ds(start + WIN, WIN), :]
-        prev_doc = docs_ext[0:1, pl.ds(start, WIN)].astype(F32)
-        this_doc = docs_ext[0:1, pl.ds(start + WIN, WIN)].astype(F32)
+        prev_doc = docs_ext[0:1, pl.ds(start, WIN)]
+        this_doc = docs_ext[0:1, pl.ds(start + WIN, WIN)]
         prev_ok = (query_doc == prev_doc) & (lane > line) & (sp * rows + b * WIN > 0)
         this_ok = (query_doc == this_doc) & (lane <= line)
         bias = jnp.concatenate(
@@ -437,36 +504,39 @@
                 heads[...], proj[:, c * 512 : (c + 1) * 512], preferred_element_type=F32
             ).astype(BF16)
 
-        @pl.when(b == n_tp - 1)
-        def _():
-            plane_step(1)
-
-        for j in range(1, planes):
-            @pl.when(b == min(j, n_tp - 1))
-            def _():
-                service("col", 0, j)
+        @pl.when(j == 0)
+        def _():
+            pair_copy(0, 2 * (1 - x) + 1 - core).start()
+
+        @pl.when(j == 1)
+        def _():
+            pair_copy(1, sibling).start()
+
+        @pl.when(j == 2)
+        def _():
+            pair_copy(0, facing).wait_recv()
+            parts[facing] = (parts[facing].astype(F32) + parts_in[0].astype(F32)).astype(BF16)
+            facing_copy().start()
 
         return carry
 
     lax.fori_loop(0, n_tp, attend_block, 0)
 
-    def rows_copy(peer, source):
-        return pltpu.make_async_remote_copy(
-            src_ref=parts.at[peer],
-            dst_ref=parts_in.at[source],
-            send_sem=rows_send.at[peer],
-            recv_sem=rows_recv.at[source],
-            device_id=(sp, peer),
-            device_id_type=MESH,
-        )
-
-    for peer in peers:
-        rows_copy(peer, tp).start()
-    for peer in peers:
-        rows_copy(peer, peer).wait_recv()
+    @pl.when(home)
+    def _():
+        for q in range(CHUNKS):
+            col(0, 1, q)
+        for q in range(CHUNKS):
+            row(0, 0, q)
+        for q in range(CHUNKS):
+            row(1, 0, q)
+
+    own_row(2)
+    own_core(2)
+    pair_copy(1, tp).wait_recv()
+    facing_copy().wait_recv()
     first = mix_scale * rest[...].astype(F32) + parts[tp].astype(F32)
-    for peer in peers:
-        first = first + parts_in[peer].astype(F32)
+    first = first + parts_in[1].astype(F32) + parts_in[2].astype(F32)
     mean = jnp.mean(first, axis=1, keepdims=True)
     first = first - mean
     var = jnp.mean(first * first, axis=1, keepdims=True)
@@ -519,20 +589,32 @@
 
     own_workers = workers(sp)
     next_workers = workers(after)
-    for i, device in enumerate(own_workers):
-        @pl.when(jnp.logical_not(is_me(device)))
-        def _():
-            norm_copy(i, device, tp).start()
 
     @pl.when(tp == n_tp - 1)
     def _():
         for i, device in enumerate(next_workers):
             tail_copy(i, device).start()
 
+    for i, device in enumerate(own_workers):
+        @pl.when(jnp.logical_not(is_me(device)))
+        def _():
+            norm_copy(i, device, tp).start()
+
+    far_sends(1, jnp.logical_not(inner))
+    near_sends(2)
+    far_sends(2, True)
     for i, peer in enumerate(peers):
         cols_copy(i, peer, tp).start()
-    service("col", 1, 1)
-    plane_step(2)
+
+    docs_copy = pltpu.make_async_remote_copy(
+        src_ref=docs_ext,
+        dst_ref=docs_other,
+        send_sem=halo_send.at[3],
+        recv_sem=halo_recv.at[3],
+        device_id=(partner, tp),
+        device_id_type=MESH,
+    )
+    docs_copy.start()
 
     @pl.when(home)
     def _():
@@ -541,18 +623,54 @@
     norm_cols[pl.ds(pl.multiple_of(tp * row_share, row_share), row_share), :] = norm_own[
         :, pl.ds(pl.multiple_of(tp * share, share), share)
     ]
-    for j in range(planes):
-        service("row", 0, j)
-    for j in range(2, planes):
-        service("col", 1, j)
-    service("own", 2, 0)
-    for j in range(planes):
-        service("row", 1, j)
+
+    @pl.when(home)
+    def _():
+        for q in range(CHUNKS):
+            col(0, 2, q)
+            col(0, 3, q)
+        for q in range(CHUNKS):
+            col(1, 1, q)
+        for q in range(CHUNKS):
+            row(0, 1, q)
+        for q in range(CHUNKS):
+            col(1, 2, q)
+            row(0, 2, q)
+            row(0, 3, q)
+        for q in range(CHUNKS):
+            row(1, 1, q)
+        for q in range(CHUNKS):
+            col(1, 3, q)
+        for q in range(CHUNKS):
+            col(2, 1, q)
+        for q in range(CHUNKS):
+            row(1, 2, q)
+            row(1, 3, q)
+
     docs_copy.wait_recv()
-    for b in range(rows // LANES + 1):
-        part = slice(b * LANES, (b + 1) * LANES)
-        row = jnp.where(home, docs_ext[0:1, part], docs_other[0:1, part]).astype(F32)
-        work_cols[part, :] = jnp.broadcast_to(row, (LANES, LANES)).T
+    place = lax.broadcasted_iota(jnp.int32, (LANES, LANES), 0)
+    for b in range(rows // LANES):
+        def columns(lag):
+            at = pl.ds(WIN + b * LANES - lag, LANES)
+            return at
+
+        now = slice(WIN + b * LANES, WIN + (b + 1) * LANES)
+        before = slice(b * LANES, (b + 1) * LANES)
+        doc_now = jnp.where(home, docs_ext[0:1, now], docs_other[0:1, now])
+        doc_before = jnp.where(home, docs_ext[0:1, before], docs_other[0:1, before])
+        tall = jnp.broadcast_to(doc_now, (LANES, LANES)).T
+        ahead = jnp.broadcast_to(doc_before, (LANES, LANES)).T
+        mask_cols[0, PAD + b * LANES : PAD + (b + 1) * LANES, :] = tall
+        if b == 0:
+            mask_cols[0, 0:PAD, :] = ahead[LANES - PAD :]
+    for b in range(rows // LANES):
+        at = PAD + b * LANES
+        doc = mask_cols[0, at : at + LANES, :]
+        for lag in range(1, TAPS):
+            same = (mask_cols[0, at - lag : at - lag + LANES, :] == doc) & (
+                place + (work * rows + b * LANES) >= lag
+            )
+            mask_cols[lag, at : at + LANES, :] = jnp.where(same, 1.0, 0.0).astype(F32)
 
     for source in range(n_tp):
         @pl.when(jnp.logical_not(home & (tp == source)))
@@ -560,6 +678,10 @@
             norm_copy(0, (sp, sibling), source).wait_recv()
 
     tail_copy(0, (sp, sibling)).wait_recv()
+
+    def await_core(w, index):
+        for q in range(CHUNKS):
+            to_core(w, index, q, slot(w, index, q)).wait_recv()
 
     @pl.when(home)
     def _():
@@ -568,21 +690,21 @@
 
     @pl.when(jnp.logical_not(home))
     def _():
-        for copy in taps:
-            copy.wait_recv()
-        for w in (0, 1):
-            for index in range(n):
-                await_block(w, index)
-
-    place = lax.broadcasted_iota(jnp.int32, (rows, LANES), 0) + work * rows
-
-    def convolved(source, taps_ref, at):
-        total = taps_ref[0:1, pl.ds(at, LANES)] * source[PAD : PAD + rows, :]
-        doc = work_cols[WIN : WIN + rows, :]
+        taps_copy.wait_recv()
+
+        def await_both(index, carry):
+            for w in (0, 1):
+                await_core(w, index)
+            return carry
+
+        lax.fori_loop(0, n, await_both, 0)
+
+    def convolved(source, first_tap, at):
+        total = taps_all[first_tap : first_tap + 1, pl.ds(at, LANES)] * source[PAD : PAD + rows, :]
         for lag in range(1, TAPS):
-            same = (work_cols[WIN - lag : WIN - lag + rows, :] == doc) & (place >= lag)
-            shifted = jnp.where(same, source[PAD - lag : PAD - lag + rows, :], 0.0)
-            total = total + taps_ref[lag : lag + 1, pl.ds(at, LANES)] * shifted
+            tap = taps_all[first_tap + lag : first_tap + lag + 1, pl.ds(at, LANES)]
+            shifted = source[PAD - lag : PAD - lag + rows, :]
+            total = total + tap * (shifted * mask_cols[lag, PAD : PAD + rows, :])
         return total
 
     def up_block(c, carry):
@@ -594,30 +716,18 @@
         both = both.astype(BF16).astype(F32)
         up_gate[...] = both[:, :LANES]
         up_value[...] = both[:, LANES:]
-        gate = convolved(up_gate, taps_gate, at)
-        value = convolved(up_value, taps_value, at)
-        inner = math.sqrt(2.0 / math.pi) * (gate + 0.044715 * (gate * gate * gate))
-        hidden[:, pl.ds(at, LANES)] = (0.5 * gate * (1.0 + jnp.tanh(inner)) * value).astype(BF16)
-        for j in range(1, planes):
-            @pl.when(c == 3 * j - 2)
+        gate = convolved(up_gate, 0, at)
+        value = convolved(up_value, TAPS, at)
+        inside = math.sqrt(2.0 / math.pi) * (gate + 0.044715 * (gate * gate * gate))
+        hidden[:, pl.ds(at, LANES)] = (0.5 * gate * (1.0 + jnp.tanh(inside)) * value).astype(BF16)
+        for q in range(CHUNKS):
+            @pl.when(home & (c == 2 * q + 1))
             def _():
-                service("col", 2, j)
-
-        for j in (0, 1):
-            @pl.when(c == 6 + 2 * j)
-            def _():
-                service("row", 2, j)
+                row(2, 0, q)
 
         return carry
 
     lax.fori_loop(0, ff // LANES, up_block, 0)
-    for j in range(2, planes):
-        service("row", 2, j)
-
-    @pl.when(jnp.logical_not(home))
-    def _():
-        for index in range(n):
-            await_block(2, index)
 
     def term_copy(index, source):
         owner = index // per
@@ -630,8 +740,22 @@
             device_id_type=MESH,
         )
 
-    def down_block(q, carry):
-        index = lax.rem(q + per * 2 * (1 - x), n)
+    def down_block(k, flip):
+        index = 2 * zone(k) + (1 - y if flip else y)
+
+        @pl.when(home)
+        def _():
+            if k > 0 and not flip and k > 1:
+                for q in range(CHUNKS):
+                    col(2, k, q)
+            if k > 0 and flip:
+                for q in range(CHUNKS):
+                    row(2, k, q)
+
+        @pl.when(jnp.logical_not(home))
+        def _():
+            await_core(2, index)
+
         terms[index] = jnp.dot(
             hidden[...], down_all[index], preferred_element_type=F32
         ).astype(BF16)
@@ -646,9 +770,8 @@
         def _():
             term_copy(index, unit).start()
 
-        return carry
-
-    lax.fori_loop(0, n, down_block, 0)
+    for k, flip in ((0, 0), (0, 1), (1, 0), (1, 1), (2, 0), (3, 0), (2, 1), (3, 1)):
+        down_block(k, flip)
 
     for source in range(n_tp):
         @pl.when(jnp.logical_not(home & (tp == source)))
@@ -691,6 +814,56 @@
 
     for peer in peers:
         stat_copy(peer, tp).start()
+
+    for w in range(3):
+        for i in range(2):
+            @pl.when(core + 2 * i != z)
+            def _():
+                for q in range(CHUNKS):
+                    to_plane(w, i, q).wait_send()
+
+    @pl.when(home)
+    def _():
+        def drain(index, carry):
+            for w in range(3):
+                for q in range(CHUNKS):
+                    to_core(w, index, q, slot(w, index, q)).wait_send()
+            return carry
+
+        lax.fori_loop(0, n, drain, 0)
+
+        def drain_rows(at, carry):
+            for w in range(3):
+                for q in range(CHUNKS):
+                    to_row(w, at, q, slot(w, 2 * at + y, q)).wait_send()
+            return carry
+
+        lax.fori_loop(0, planes, drain_rows, 0)
+        taps_copy.wait_send()
+
+    for copy in halo:
+        copy.wait_send()
+    docs_copy.wait_send()
+    for i, device in enumerate(own_workers):
+        @pl.when(jnp.logical_not(is_me(device)))
+        def _():
+            norm_copy(i, device, tp).wait_send()
+
+    @pl.when(tp == n_tp - 1)
+    def _():
+        for i, device in enumerate(next_workers):
+            tail_copy(i, device).wait_send()
+
+    pair_copy(0, 2 * (1 - x) + 1 - core).wait_send()
+    pair_copy(1, sibling).wait_send()
+    facing_copy().wait_send()
+    for i, peer in enumerate(peers):
+        cols_copy(i, peer, tp).wait_send()
+    for index in range(n):
+        @pl.when(jnp.logical_not(home & (tp == index // per)))
+        def _():
+            term_copy(index, unit).wait_send()
+
     for peer in peers:
         stat_copy(peer, peer).wait_recv()
     total = stats[0]
@@ -702,40 +875,8 @@
     out_ref[...] = (
         (second[...] - mean) * lax.rsqrt(var + norm_eps) * final_ref[...]
     ).astype(BF16)
-
-    plane_step(3)
-
-    @pl.when(home)
-    def _():
-        for w in range(3):
-            for at in range(planes):
-                to_row(w, at, slot(w, sp)).wait_send()
-            for index in range(n):
-                to_core(w, index, slot(w, index)).wait_send()
-        for copy in taps:
-            copy.wait_send()
-
-    for copy in halo:
-        copy.wait_send()
-    docs_copy.wait_send()
-    for i, device in enumerate(own_workers):
-        @pl.when(jnp.logical_not(is_me(device)))
-        def _():
-            norm_copy(i, device, tp).wait_send()
-
-    @pl.when(tp == n_tp - 1)
-    def _():
-        for i, device in enumerate(next_workers):
-            tail_copy(i, device).wait_send()
-
-    for i, peer in enumerate(peers):
-        rows_copy(peer, tp).wait_send()
-        cols_copy(i, peer, tp).wait_send()
+    for peer in peers:
         stat_copy(peer, tp).wait_send()
-    for index in range(n):
-        @pl.when(jnp.logical_not(home & (tp == index // per)))
-        def _():
-            term_copy(index, unit).wait_send()
 
 
 def fused(
@@ -762,8 +903,11 @@
     cols = down_proj.shape[1]
     per = width // n_tp // cols
     planes = n // 2
-    kv = jnp.concatenate([key_rows, value_rows, value_rows, key_rows], axis=1)
-    docs = jnp.broadcast_to(doc_ids[None, :], (8, rows))
+    taps = jnp.concatenate(
+        [gate_taps, value_taps, jnp.zeros((8 - 2 * TAPS, ff), F32)], axis=0
+    )
+    docs = jnp.broadcast_to(doc_ids.astype(F32)[None, :], (8, rows))
+    aux = jnp.concatenate([taps, docs], axis=1)
     share = rows // n_tp
     anywhere = pl.BlockSpec(memory_space=pl.ANY)
     vmem = pl.BlockSpec(memory_space=pltpu.VMEM)
@@ -773,27 +917,27 @@
         functools.partial(layer_kernel, n, n_tp),
         out_shape=jax.ShapeDtypeStruct((rows, width // n_tp), BF16),
         in_specs=[
-            anywhere, anywhere, smem, anywhere, anywhere, anywhere, vmem,
-            anywhere, anywhere, anywhere, anywhere, anywhere, vmem,
+            anywhere, anywhere, anywhere, smem, anywhere, anywhere, anywhere, vmem,
+            anywhere, anywhere, anywhere, vmem,
         ],
         out_specs=vmem,
         scratch_shapes=[
             pltpu.VMEM((n * depth, ff), BF16),
             pltpu.VMEM((n * depth, ff), BF16),
             pltpu.VMEM((n, ff, cols), BF16),
-            pltpu.VMEM((WIN + rows, 4 * HD), BF16),
-            pltpu.VMEM((8, WIN + rows), jnp.int32),
-            pltpu.VMEM((8, WIN + rows), jnp.int32),
+            pltpu.VMEM((WIN + rows, HD), BF16),
+            pltpu.VMEM((WIN + rows, HD), BF16),
+            pltpu.VMEM((8, WIN + rows), F32),
+            pltpu.VMEM((8, WIN + rows), F32),
             pltpu.VMEM((WIN + rows, LANES), F32),
-            pltpu.VMEM((WIN + rows, LANES), F32),
-            pltpu.VMEM(gate_taps.shape, F32),
-            pltpu.VMEM(gate_taps.shape, F32),
+            pltpu.VMEM((TAPS, PAD + rows, LANES), F32),
+            pltpu.VMEM((8, ff), F32),
             pltpu.VMEM((rows, head_cols), BF16),
             pltpu.VMEM((head_cols, width), BF16),
             pltpu.VMEM((share, width), BF16),
             pltpu.VMEM((share, head_cols), BF16),
             pltpu.VMEM((n_tp, share, width), BF16),
-            pltpu.VMEM((n_tp, share, width), BF16),
+            pltpu.VMEM((3, share, width), BF16),
             pltpu.VMEM((share, width), BF16),
             pltpu.VMEM((rows, width // n_tp), BF16),
             pltpu.VMEM((PAD + rows, width), BF16),
@@ -804,17 +948,18 @@
             pltpu.VMEM((n_tp, per, rows, cols), BF16),
             pltpu.VMEM((rows, width // n_tp), F32),
             pltpu.VMEM((n_tp, 8, rows), F32),
-            dma((3, planes // 2)),
-            dma((3, planes)),
-            dma((3, n)),
-            dma((3, n)),
+            dma((3, 2, CHUNKS)),
+            dma((3, planes, CHUNKS)),
+            dma((3, n, CHUNKS)),
+            dma((3, n, CHUNKS)),
+            dma((3, n, CHUNKS)),
             dma((10,)),
-            dma((2,)),
-            dma((2,)),
+            dma(()),
+            dma(()),
+            dma((4,)),
+            dma((4,)),
             dma((3,)),
             dma((3,)),
-            dma((n_tp,)),
-            dma((n_tp,)),
             dma((n_tp,)),
             dma((n_tp,)),
             dma((n_tp,)),
@@ -831,8 +976,9 @@
         ),
         name="layer",
     )(
-        kv,
-        docs,
+        key_rows,
+        value_rows,
+        aux,
         sink_logit,
         query_rows,
         out_proj,
@@ -840,8 +986,6 @@
         mix_gain[None, :],
         gate_proj,
         value_proj,
-        gate_taps,
-        value_taps,
         down_proj,
         final_gain[None, :],
     )
@@ -854,16 +998,15 @@
     depth, ff = gate_proj.shape
     cols = down_proj.shape[1]
     fits = (
-        n % 4 == 0
+        n == 8
         and n_tp == 4
-        and n >= 8
-        and n <= n_tp * 2
         and ff >= 10 * LANES
         and query_rows.shape[0] == n_tp * WIN
         and key_rows.shape[1] == HD
         and query_rows.shape[1] % LANES == 0
-        and depth % 32 == 0
+        and depth % (16 * CHUNKS) == 0
         and ff % LANES == 0
+        and ff % (16 * CHUNKS) == 0
         and cols % LANES == 0
         and share % cols == 0
     )

time: 180 us -> 159 us (0.88); the launches traced: 177 us -> 158 us
  Pallas kernels: 171 us -> 151 us
    pallas_call x1, Pallas kernels: 171 us -> 151 us  [fused(): pl.pallas_call(functools.partial(layer_kernel, n, n_tp), out_shape=jax.Sh...]
where the time goes in v1:
time: 159 us; the launch traced here: 158 us
  Pallas kernels  151 us (95%)
  local copies, waits for them, and re-layouts  5.07 us (3%)
  other arithmetic  2.07 us (1%)
    pallas_call x1, Pallas kernels, fused(): pl.pallas_call(functools.partial(layer_kernel, n, n_tp), out_shape=jax.Sh...  151 us
    unnamed x3, local copies, waits for them, and re-layouts  5.06 us

profile of v1, /device:TPU:0, one launch (start us, length us, event | category | flops | bytes accessed | tf_op | source)
XLA Modules:
  0.0 158.2 jit_solution(997203408832327347)
XLA Ops:
  0.0 0.7 convert_element_type.3
  0.7 1.4 maximum_maximum_fusion.aux_ref
  2.1 1.6 %copy.15.key_ref = bf16[512,64]{1,0:T(8,128)(2,1)} copy(bf16[512,64]{0,1:T(8,128)(2,1)} %param.15) | data formatting | bytes 131072 | tf_op args[1]
  3.7 1.6 %copy.16.val_ref = bf16[512,64]{1,0:T(8,128)(2,1)} copy(bf16[512,64]{0,1:T(8,128)(2,1)} %param.16) | data formatting | bytes 131072 | tf_op args[2]
  5.3 151.1 %layer.1 = bf16[512,512]{1,0:T(8,128)(2,1)} custom-call(bf16[512,64]{1,0:T(8,128)(2,1)} %copy.15.key_ref, bf16[512,64]{1,0:T(8,128)(2,1)} %copy.16.val_ref, f32[8,1920]{1,0:T(8,128)} %maximum_maximum_fusion.aux_ref, f32[8]{0:T(128)} %sink_ref.1, bf16[512,512]{1,0:T(8,128)(2,1)} %query_ref.1, bf16[512,2048]{1,0:T(8,128)(2,1)} %out_proj_ref.1, ...), custom_call_target="tpu_custom_call" | custom-call | tf_op jit(solution)/shard_map/layer/pallas_call | solution.py:916
  156.4 1.9 %copy.18 = bf16[512,512]{1,0:T(8,128)(2,1)} copy(bf16[512,512]{1,0:T(8,128)(2,1)} %layer.1) | data formatting | bytes 1048576
  (2 shorter events, 0.0 us)

commit v2 on v1

--- a/solution.py
+++ b/solution.py
@@ -146,6 +146,31 @@
 LANES = 128
 PAD = 16
 CHUNKS = 4
+PAIR = (0, 1)
+EARLY = (
+    [("col", 0, 1, i) for i in PAIR]
+    + [("far", 1, 0, 0)]
+    + [("row", 0, 0, i) for i in PAIR]
+    + [("row", 1, 0, i) for i in PAIR]
+)
+MIDDLE = (
+    [("col", 1, 1, i) for i in PAIR]
+    + [("far", 2, 0, 0)]
+    + [("col", 2, 1, i) for i in PAIR]
+    + [("row", 2, 0, i) for i in PAIR]
+    + [(kind, 0, k, i) for i in PAIR for kind, k in (("col", 2), ("col", 3), ("row", 1))]
+    + [("norm", 0, 0, 0)]
+    + [("row", 1, 1, i) for i in PAIR]
+    + [(kind, w, k, i) for i in PAIR for w, kind, k in ((1, "col", 2), (0, "row", 2), (1, "col", 3), (0, "row", 3))]
+    + [("row", 1, k, i) for i in PAIR for k in (2, 3)]
+)
+UP_SERVE = ((2, [("row", 2, 1, 0)]), (4, [("row", 2, 1, 1)]))
+DOWN_SERVE = {
+    (2, 0): [("col", 2, 2, i) for i in PAIR],
+    (3, 0): [("col", 2, 3, i) for i in PAIR],
+    (2, 1): [("row", 2, 2, i) for i in PAIR],
+    (3, 1): [("row", 2, 3, i) for i in PAIR],
+}
 F32 = jnp.float32
 BF16 = jnp.bfloat16
 
@@ -155,7 +180,7 @@
     n_tp,
     key_ref,
     val_ref,
-    aux_ref,
+    docs_ref,
     sink_ref,
     query_ref,
     out_proj_ref,
@@ -163,6 +188,8 @@
     mix_ref,
     gate_ref,
     value_ref,
+    gate_taps_ref,
+    value_taps_ref,
     down_ref,
     final_ref,
     out_ref,
@@ -175,7 +202,8 @@
     docs_other,
     doc_cols,
     mask_cols,
-    taps_all,
+    taps_gate,
+    taps_value,
     queries,
     proj,
     rest,
@@ -193,6 +221,7 @@
     second,
     stats,
     plane_send,
+    onward_send,
     row_send,
     core_send,
     block_recv,
@@ -206,6 +235,7 @@
     rows_recv,
     norm_send,
     norm_recv,
+    pass_send,
     cols_send,
     cols_recv,
     tail_send,
@@ -257,10 +287,9 @@
         return carry
 
     lax.fori_loop(1, everyone, greet, 0)
-    docs_ref = aux_ref.at[:, pl.ds(ff, rows)]
     fetch = [
-        pltpu.make_async_copy(key_ref, key_ext.at[pl.ds(WIN, rows)], local_sem.at[0]),
-        pltpu.make_async_copy(val_ref, val_ext.at[pl.ds(WIN, rows)], local_sem.at[1]),
+        pltpu.make_async_copy(key_ref, key_ext.at[:, pl.ds(WIN, rows)], local_sem.at[0]),
+        pltpu.make_async_copy(val_ref, val_ext.at[:, pl.ds(WIN, rows)], local_sem.at[1]),
         pltpu.make_async_copy(docs_ref, docs_ext.at[:, pl.ds(WIN, rows)], local_sem.at[2]),
         pltpu.make_async_copy(query_ref, queries, local_sem.at[3]),
         pltpu.make_async_copy(out_proj_ref, proj, local_sem.at[4]),
@@ -299,17 +328,17 @@
             dst_ref=slot(w, sp, q),
             send_sem=plane_send.at[w, i, q],
             recv_sem=block_recv.at[w, sp, q],
-            device_id=(2 * (core + 2 * i) + y, tp),
-            device_id_type=MESH,
-        )
-
-    def to_row(w, at, q, source):
+            device_id=(2 * (core + 2 * i) + y, 2 * x + (core if q % 2 == 0 else 1 - core)),
+            device_id_type=MESH,
+        )
+
+    def to_row(w, at, q, source, target):
         return pltpu.make_async_remote_copy(
             src_ref=source,
             dst_ref=slot(w, 2 * at + y, q),
             send_sem=row_send.at[w, at, q],
             recv_sem=block_recv.at[w, 2 * at + y, q],
-            device_id=(across, tp),
+            device_id=(across, target),
             device_id_type=MESH,
         )
 
@@ -356,7 +385,7 @@
         @pl.when(home)
         def _():
             for q in range(CHUNKS):
-                to_row(w, z, q, piece(w, q)).start()
+                to_row(w, z, q, piece(w, q), tp if q % 2 == 0 else sibling).start()
 
     def own_core(w):
         @pl.when(home)
@@ -364,17 +393,61 @@
             for q in range(CHUNKS):
                 to_core(w, sp, q, piece(w, q)).start()
 
-    def col(w, k, q):
-        at = zone(k)
+    role = jnp.where(home, 0, 1)
+
+    def onward(w, i):
+        index, q = 2 * zone(1) + y, 2 * i + role
+        return pltpu.make_async_remote_copy(
+            src_ref=slot(w, index, q),
+            dst_ref=slot(w, index, q),
+            send_sem=onward_send.at[w, i],
+            recv_sem=block_recv.at[w, index, q],
+            device_id=(2 * (z + 2 - 4 * half) + y, tp),
+            device_id_type=MESH,
+        )
+
+    def col(w, k, i):
+        at, q = zone(k), 2 * i + role
         index = 2 * at + y
         await_piece(w, index, q)
-        to_row(w, at, q, slot(w, index, q)).start()
+        if k == 1:
+            @pl.when(inner)
+            def _():
+                onward(w, i).start()
+
+        to_row(w, at, q, slot(w, index, q), tp).start()
         to_core(w, index, q, slot(w, index, q)).start()
 
-    def row(w, k, q):
-        index = 2 * zone(k) + 1 - y
+    def row(w, k, i):
+        index, q = 2 * zone(k) + 1 - y, 2 * i + role
         await_piece(w, index, q)
         to_core(w, index, q, slot(w, index, q)).start()
+
+    def serve(events):
+        for kind, w, k, i in events:
+            if kind == "far":
+                far_sends(w, inner)
+            elif kind == "norm":
+                @pl.when(jnp.logical_not(home))
+                def _():
+                    for i in PAIR:
+                        norm_copy(0, (sp, sibling), 2 * x + i).wait_recv()
+                        norm_pass(i).start()
+
+            else:
+                (col if kind == "col" else row)(w, k, i)
+
+    def await_slab(w, k, flip):
+        index = 2 * zone(k) + (1 - y if flip else y)
+        if k == 0 and not flip:
+            @pl.when(jnp.logical_not(home))
+            def _():
+                for q in range(CHUNKS):
+                    to_core(w, index, q, slot(w, index, q)).wait_recv()
+        else:
+            for i in range(CHUNKS // 2):
+                q = 2 * i + 1 - role
+                to_core(w, index, q, slot(w, index, q)).wait_recv()
 
     halo = [
         pltpu.make_async_remote_copy(
@@ -387,56 +460,60 @@
         )
         for i, (source, target) in enumerate(
             (
-                (key_ref.at[pl.ds(rows - WIN, WIN)], key_ext.at[pl.ds(0, WIN)]),
-                (val_ref.at[pl.ds(rows - WIN, WIN)], val_ext.at[pl.ds(0, WIN)]),
-                (
-                    aux_ref.at[:, pl.ds(ff + rows - WIN, WIN)],
-                    docs_ext.at[:, pl.ds(0, WIN)],
-                ),
+                (ref.at[:, pl.ds(rows - WIN, WIN)], ext.at[:, pl.ds(0, WIN)])
+                for ref, ext in (
+                    (key_ref, key_ext),
+                    (val_ref, val_ext),
+                    (docs_ref, docs_ext),
+                )
             )
         )
     ]
     for copy in halo:
         copy.start()
     near_sends(0)
-    far_sends(0, True)
+    far_sends(0, inner | home)
+    near_sends(1)
+    near_sends(2)
     own_row(0)
     own_row(1)
-    near_sends(1)
-    far_sends(1, inner)
+    own_row(2)
     settle = [
         pltpu.make_async_copy(own[w], slab(w, sp), local_sem.at[6 + w]) for w in range(3)
     ]
-    settle.append(
-        pltpu.make_async_copy(aux_ref.at[:, pl.ds(0, ff)], taps_all, local_sem.at[9])
-    )
-    taps_copy = pltpu.make_async_remote_copy(
-        src_ref=aux_ref.at[:, pl.ds(0, ff)],
-        dst_ref=taps_all,
-        send_sem=taps_send,
-        recv_sem=taps_recv,
-        device_id=(sp, sibling),
-        device_id_type=MESH,
-    )
+    tap_pairs = ((gate_taps_ref, taps_gate), (value_taps_ref, taps_value))
+    for i, (source, target) in enumerate(tap_pairs):
+        settle.append(pltpu.make_async_copy(source, target, local_sem.at[9 + i]))
+    taps = [
+        pltpu.make_async_remote_copy(
+            src_ref=source,
+            dst_ref=target,
+            send_sem=taps_send.at[i],
+            recv_sem=taps_recv.at[i],
+            device_id=(sp, sibling),
+            device_id_type=MESH,
+        )
+        for i, (source, target) in enumerate(tap_pairs)
+    ]
 
     @pl.when(home)
     def _():
-        for copy in settle:
+        for copy in settle + taps:
             copy.start()
-        taps_copy.start()
 
     own_core(0)
     own_core(1)
+    own_core(2)
     for copy in fetch:
         copy.wait()
 
     line = lax.broadcasted_iota(jnp.int32, (LANES, LANES), 0)
     lane = lax.broadcasted_iota(jnp.int32, (LANES, LANES), 1)
     for b in range(1, rows // LANES + 1):
-        row_doc = docs_ext[0:1, b * LANES : (b + 1) * LANES]
+        row_doc = docs_ext[0:1, b * LANES : (b + 1) * LANES].astype(F32)
         doc_cols[b * LANES : (b + 1) * LANES, :] = jnp.broadcast_to(row_doc, (LANES, LANES)).T
 
-    zero = jnp.zeros((2 * WIN, HD), BF16)
+    zero = jnp.zeros((HD, 2 * WIN), BF16)
 
     def pair_copy(i, block):
         return pltpu.make_async_remote_copy(
@@ -467,8 +544,8 @@
                 copy.wait_recv()
 
         start = pl.multiple_of(b * WIN, WIN)
-        k = key_ext[pl.ds(start, 2 * WIN), :]
-        v = val_ext[pl.ds(start, 2 * WIN), :]
+        k = key_ext[:, pl.ds(start, 2 * WIN)]
+        v = val_ext[:, pl.ds(start, 2 * WIN)]
         keys = jnp.concatenate(
             [jnp.concatenate([k, zero], axis=1), jnp.concatenate([zero, k], axis=1)], axis=0
         )
@@ -476,8 +553,8 @@
             [jnp.concatenate([v, zero], axis=1), jnp.concatenate([zero, v], axis=1)], axis=0
         )
         query_doc = doc_cols[pl.ds(start + WIN, WIN), :]
-        prev_doc = docs_ext[0:1, pl.ds(start, WIN)]
-        this_doc = docs_ext[0:1, pl.ds(start + WIN, WIN)]
+        prev_doc = docs_ext[0:1, pl.ds(start, WIN)].astype(F32)
+        this_doc = docs_ext[0:1, pl.ds(start + WIN, WIN)].astype(F32)
         prev_ok = (query_doc == prev_doc) & (lane > line) & (sp * rows + b * WIN > 0)
         this_ok = (query_doc == this_doc) & (lane <= line)
         bias = jnp.concatenate(
@@ -485,9 +562,7 @@
         ).astype(F32)
         for pair in range(query_ref.shape[1] // LANES):
             block = queries[pl.ds(start, WIN), pair * LANES : (pair + 1) * LANES]
-            both = lax.dot_general(
-                block, keys, (((1,), (1,)), ((), ())), preferred_element_type=F32
-            )
+            both = jnp.dot(block, keys, preferred_element_type=F32)
             probs = []
             for side in (0, 1):
                 scores = both[:, side * 2 * WIN : (side + 1) * 2 * WIN] * HD ** (-0.5) + bias
@@ -496,8 +571,11 @@
                 weights = jnp.exp(scores - top)
                 total = jnp.sum(weights, axis=1, keepdims=True) + jnp.exp(sink - top)
                 probs.append((weights / total).astype(BF16))
-            heads[:, pair * LANES : (pair + 1) * LANES] = jnp.dot(
-                jnp.concatenate(probs, axis=1), values, preferred_element_type=F32
+            heads[:, pair * LANES : (pair + 1) * LANES] = lax.dot_general(
+                jnp.concatenate(probs, axis=1),
+                values,
+                (((1,), (1,)), ((), ())),
+                preferred_element_type=F32,
             ).astype(BF16)
         for c in range(width // 512):
             parts[b, :, c * 512 : (c + 1) * 512] = jnp.dot(
@@ -522,17 +600,7 @@
 
     lax.fori_loop(0, n_tp, attend_block, 0)
 
-    @pl.when(home)
-    def _():
-        for q in range(CHUNKS):
-            col(0, 1, q)
-        for q in range(CHUNKS):
-            row(0, 0, q)
-        for q in range(CHUNKS):
-            row(1, 0, q)
-
-    own_row(2)
-    own_core(2)
+    serve(EARLY)
     pair_copy(1, tp).wait_recv()
     facing_copy().wait_recv()
     first = mix_scale * rest[...].astype(F32) + parts[tp].astype(F32)
@@ -563,8 +631,18 @@
             device_id_type=MESH,
         )
 
-    def is_me(device):
-        return (device[0] == sp) & (device[1] == tp)
+    def takes(i, device):
+        return jnp.where(device[0] == sp, device[1] != tp, x == i % 2)
+
+    def norm_pass(i):
+        return pltpu.make_async_remote_copy(
+            src_ref=normed.at[place_of(2 * x + i)],
+            dst_ref=normed.at[place_of(2 * x + i)],
+            send_sem=pass_send.at[i],
+            recv_sem=norm_recv.at[2 * x + i],
+            device_id=(sp, facing),
+            device_id_type=MESH,
+        )
 
     def cols_copy(i, peer, source):
         rows_at = pl.ds(pl.multiple_of(source * row_share, row_share), row_share)
@@ -579,8 +657,8 @@
 
     def tail_copy(i, device):
         return pltpu.make_async_remote_copy(
-            src_ref=norm_own.at[pl.ds(row_share - PAD, PAD)],
-            dst_ref=normed.at[pl.ds(0, PAD)],
+            src_ref=norm_own.at[pl.ds(row_share - PAD // 2, PAD // 2)],
+            dst_ref=normed.at[pl.ds(PAD // 2, PAD // 2)],
             send_sem=tail_send.at[i],
             recv_sem=tail_recv,
             device_id=device,
@@ -590,19 +668,18 @@
     own_workers = workers(sp)
     next_workers = workers(after)
 
-    @pl.when(tp == n_tp - 1)
+    @pl.when((tp == n_tp - 1) & (sp < n - 1))
     def _():
         for i, device in enumerate(next_workers):
             tail_copy(i, device).start()
 
     for i, device in enumerate(own_workers):
-        @pl.when(jnp.logical_not(is_me(device)))
+        @pl.when(takes(i, device))
         def _():
             norm_copy(i, device, tp).start()
 
-    far_sends(1, jnp.logical_not(inner))
-    near_sends(2)
-    far_sends(2, True)
+    far_sends(1, home & jnp.logical_not(inner))
+    far_sends(2, home & jnp.logical_not(inner))
     for i, peer in enumerate(peers):
         cols_copy(i, peer, tp).start()
 
@@ -624,40 +701,14 @@
         :, pl.ds(pl.multiple_of(tp * share, share), share)
     ]
 
-    @pl.when(home)
-    def _():
-        for q in range(CHUNKS):
-            col(0, 2, q)
-            col(0, 3, q)
-        for q in range(CHUNKS):
-            col(1, 1, q)
-        for q in range(CHUNKS):
-            row(0, 1, q)
-        for q in range(CHUNKS):
-            col(1, 2, q)
-            row(0, 2, q)
-            row(0, 3, q)
-        for q in range(CHUNKS):
-            row(1, 1, q)
-        for q in range(CHUNKS):
-            col(1, 3, q)
-        for q in range(CHUNKS):
-            col(2, 1, q)
-        for q in range(CHUNKS):
-            row(1, 2, q)
-            row(1, 3, q)
-
+    serve(MIDDLE)
     docs_copy.wait_recv()
     place = lax.broadcasted_iota(jnp.int32, (LANES, LANES), 0)
     for b in range(rows // LANES):
-        def columns(lag):
-            at = pl.ds(WIN + b * LANES - lag, LANES)
-            return at
-
         now = slice(WIN + b * LANES, WIN + (b + 1) * LANES)
         before = slice(b * LANES, (b + 1) * LANES)
-        doc_now = jnp.where(home, docs_ext[0:1, now], docs_other[0:1, now])
-        doc_before = jnp.where(home, docs_ext[0:1, before], docs_other[0:1, before])
+        doc_now = jnp.where(home, docs_ext[0:1, now], docs_other[0:1, now]).astype(F32)
+        doc_before = jnp.where(home, docs_ext[0:1, before], docs_other[0:1, before]).astype(F32)
         tall = jnp.broadcast_to(doc_now, (LANES, LANES)).T
         ahead = jnp.broadcast_to(doc_before, (LANES, LANES)).T
         mask_cols[0, PAD + b * LANES : PAD + (b + 1) * LANES, :] = tall
@@ -673,15 +724,18 @@
             mask_cols[lag, at : at + LANES, :] = jnp.where(same, 1.0, 0.0).astype(F32)
 
     for source in range(n_tp):
-        @pl.when(jnp.logical_not(home & (tp == source)))
+        @pl.when(jnp.where(home, tp != source, x != source // 2))
         def _():
             norm_copy(0, (sp, sibling), source).wait_recv()
 
-    tail_copy(0, (sp, sibling)).wait_recv()
-
-    def await_core(w, index):
-        for q in range(CHUNKS):
-            to_core(w, index, q, slot(w, index, q)).wait_recv()
+    @pl.when(work > 0)
+    def _():
+        tail_copy(0, (sp, sibling)).wait_recv()
+
+    @pl.when(work == 0)
+    def _():
+        normed[0:PAD, :] = jnp.zeros((PAD, width), BF16)
+
 
     @pl.when(home)
     def _():
@@ -690,19 +744,18 @@
 
     @pl.when(jnp.logical_not(home))
     def _():
-        taps_copy.wait_recv()
-
-        def await_both(index, carry):
-            for w in (0, 1):
-                await_core(w, index)
-            return carry
-
-        lax.fori_loop(0, n, await_both, 0)
-
-    def convolved(source, first_tap, at):
-        total = taps_all[first_tap : first_tap + 1, pl.ds(at, LANES)] * source[PAD : PAD + rows, :]
+        for copy in taps:
+            copy.wait_recv()
+
+    for w in (0, 1):
+        for k in range(planes):
+            for flip in (0, 1):
+                await_slab(w, k, flip)
+
+    def convolved(source, taps_ref, at):
+        total = taps_ref[0:1, pl.ds(at, LANES)] * source[PAD : PAD + rows, :]
         for lag in range(1, TAPS):
-            tap = taps_all[first_tap + lag : first_tap + lag + 1, pl.ds(at, LANES)]
+            tap = taps_ref[lag : lag + 1, pl.ds(at, LANES)]
             shifted = source[PAD - lag : PAD - lag + rows, :]
             total = total + tap * (shifted * mask_cols[lag, PAD : PAD + rows, :])
         return total
@@ -716,14 +769,14 @@
         both = both.astype(BF16).astype(F32)
         up_gate[...] = both[:, :LANES]
         up_value[...] = both[:, LANES:]
-        gate = convolved(up_gate, 0, at)
-        value = convolved(up_value, TAPS, at)
+        gate = convolved(up_gate, taps_gate, at)
+        value = convolved(up_value, taps_value, at)
         inside = math.sqrt(2.0 / math.pi) * (gate + 0.044715 * (gate * gate * gate))
         hidden[:, pl.ds(at, LANES)] = (0.5 * gate * (1.0 + jnp.tanh(inside)) * value).astype(BF16)
-        for q in range(CHUNKS):
-            @pl.when(home & (c == 2 * q + 1))
+        for at_step, events in UP_SERVE:
+            @pl.when(c == at_step)
             def _():
-                row(2, 0, q)
+                serve(events)
 
         return carry
 
@@ -743,19 +796,8 @@
     def down_block(k, flip):
         index = 2 * zone(k) + (1 - y if flip else y)
 
-        @pl.when(home)
-        def _():
-            if k > 0 and not flip and k > 1:
-                for q in range(CHUNKS):
-                    col(2, k, q)
-            if k > 0 and flip:
-                for q in range(CHUNKS):
-                    row(2, k, q)
-
-        @pl.when(jnp.logical_not(home))
-        def _():
-            await_core(2, index)
-
+        serve(DOWN_SERVE.get((k, flip), ()))
+        await_slab(2, k, flip)
         terms[index] = jnp.dot(
             hidden[...], down_all[index], preferred_element_type=F32
         ).astype(BF16)
@@ -817,39 +859,51 @@
 
     for w in range(3):
         for i in range(2):
-            @pl.when(core + 2 * i != z)
+            @pl.when((core + 2 * i != z) & ((half == i) | inner | home))
             def _():
                 for q in range(CHUNKS):
                     to_plane(w, i, q).wait_send()
 
+        @pl.when(inner)
+        def _():
+            for i in range(CHUNKS // 2):
+                onward(w, i).wait_send()
+
+    for k in range(planes):
+        at = zone(k)
+        for w in range(3):
+            for i in range(CHUNKS // 2):
+                q = 2 * i + role
+                if k > 0:
+                    index = 2 * at + y
+                    to_row(w, at, q, slot(w, index, q), tp).wait_send()
+                    to_core(w, index, q, slot(w, index, q)).wait_send()
+                index = 2 * at + 1 - y
+                to_core(w, index, q, slot(w, index, q)).wait_send()
+
     @pl.when(home)
     def _():
-        def drain(index, carry):
-            for w in range(3):
-                for q in range(CHUNKS):
-                    to_core(w, index, q, slot(w, index, q)).wait_send()
-            return carry
-
-        lax.fori_loop(0, n, drain, 0)
-
-        def drain_rows(at, carry):
-            for w in range(3):
-                for q in range(CHUNKS):
-                    to_row(w, at, q, slot(w, 2 * at + y, q)).wait_send()
-            return carry
-
-        lax.fori_loop(0, planes, drain_rows, 0)
-        taps_copy.wait_send()
+        for w in range(3):
+            for q in range(CHUNKS):
+                to_row(w, z, q, piece(w, q), tp if q % 2 == 0 else sibling).wait_send()
+                to_core(w, sp, q, piece(w, q)).wait_send()
+        for copy in taps:
+            copy.wait_send()
 
     for copy in halo:
         copy.wait_send()
     docs_copy.wait_send()
     for i, device in enumerate(own_workers):
-        @pl.when(jnp.logical_not(is_me(device)))
+        @pl.when(takes(i, device))
         def _():
             norm_copy(i, device, tp).wait_send()
 
-    @pl.when(tp == n_tp - 1)
+    @pl.when(jnp.logical_not(home))
+    def _():
+        for i in PAIR:
+            norm_pass(i).wait_send()
+
+    @pl.when((tp == n_tp - 1) & (sp < n - 1))
     def _():
         for i, device in enumerate(next_workers):
             tail_copy(i, device).wait_send()
@@ -903,11 +957,6 @@
     cols = down_proj.shape[1]
     per = width // n_tp // cols
     planes = n // 2
-    taps = jnp.concatenate(
-        [gate_taps, value_taps, jnp.zeros((8 - 2 * TAPS, ff), F32)], axis=0
-    )
-    docs = jnp.broadcast_to(doc_ids.astype(F32)[None, :], (8, rows))
-    aux = jnp.concatenate([taps, docs], axis=1)
     share = rows // n_tp
     anywhere = pl.BlockSpec(memory_space=pl.ANY)
     vmem = pl.BlockSpec(memory_space=pltpu.VMEM)
@@ -918,20 +967,21 @@
         out_shape=jax.ShapeDtypeStruct((rows, width // n_tp), BF16),
         in_specs=[
             anywhere, anywhere, anywhere, smem, anywhere, anywhere, anywhere, vmem,
-            anywhere, anywhere, anywhere, vmem,
+            anywhere, anywhere, anywhere, anywhere, anywhere, vmem,
         ],
         out_specs=vmem,
         scratch_shapes=[
             pltpu.VMEM((n * depth, ff), BF16),
             pltpu.VMEM((n * depth, ff), BF16),
             pltpu.VMEM((n, ff, cols), BF16),
-            pltpu.VMEM((WIN + rows, HD), BF16),
-            pltpu.VMEM((WIN + rows, HD), BF16),
-            pltpu.VMEM((8, WIN + rows), F32),
-            pltpu.VMEM((8, WIN + rows), F32),
+            pltpu.VMEM((HD, WIN + rows), BF16),
+            pltpu.VMEM((HD, WIN + rows), BF16),
+            pltpu.VMEM((1, WIN + rows), jnp.int32),
+            pltpu.VMEM((1, WIN + rows), jnp.int32),
             pltpu.VMEM((WIN + rows, LANES), F32),
             pltpu.VMEM((TAPS, PAD + rows, LANES), F32),
-            pltpu.VMEM((8, ff), F32),
+            pltpu.VMEM(gate_taps.shape, F32),
+            pltpu.VMEM(value_taps.shape, F32),
             pltpu.VMEM((rows, head_cols), BF16),
             pltpu.VMEM((head_cols, width), BF16),
             pltpu.VMEM((share, width), BF16),
@@ -949,19 +999,21 @@
             pltpu.VMEM((rows, width // n_tp), F32),
             pltpu.VMEM((n_tp, 8, rows), F32),
             dma((3, 2, CHUNKS)),
+            dma((3, CHUNKS // 2)),
             dma((3, planes, CHUNKS)),
             dma((3, n, CHUNKS)),
             dma((3, n, CHUNKS)),
             dma((3, n, CHUNKS)),
-            dma((10,)),
-            dma(()),
-            dma(()),
+            dma((11,)),
+            dma((2,)),
+            dma((2,)),
             dma((4,)),
             dma((4,)),
             dma((3,)),
             dma((3,)),
             dma((n_tp,)),
             dma((n_tp,)),
+            dma((2,)),
             dma((n_tp,)),
             dma((n_tp,)),
             dma((n_tp,)),
@@ -976,9 +1028,9 @@
         ),
         name="layer",
     )(
-        key_rows,
-        value_rows,
-        aux,
+        key_rows.T,
+        value_rows.T,
+        doc_ids[None, :],
         sink_logit,
         query_rows,
         out_proj,
@@ -986,6 +1038,8 @@
         mix_gain[None, :],
         gate_proj,
         value_proj,
+        gate_taps,
+        value_taps,
         down_proj,
         final_gain[None, :],
     )

time: 159 us -> 146 us (0.918)
  Pallas kernels: 151 us -> 144 us
  local copies, waits for them, and re-layouts: 5.07 us -> 1.87 us
  other arithmetic: 2.07 us -> 0 us
    pallas_call x1, Pallas kernels: 151 us -> 144 us  [fused(): pl.pallas_call(functools.partial(layer_kernel, n, n_tp), out_shape=jax.Sh...]
    unnamed x3 -> x1, local copies, waits for them, and re-layouts: 5.06 us -> 1.87 us
where the time goes in v2:
time: 146 us; the launch traced here: 145 us
  Pallas kernels  144 us (99%)
  local copies, waits for them, and re-layouts  1.87 us (1%)
    pallas_call x1, Pallas kernels, fused(): pl.pallas_call(functools.partial(layer_kernel, n, n_tp), out_shape=jax.Sh...  144 us

profile of v2, /device:TPU:0, one launch (start us, length us, event | category | flops | bytes accessed | tf_op | source)
XLA Modules:
  0.0 145.4 jit_solution(1251273878872505324)
XLA Ops:
  0.0 143.6 %layer.1 = bf16[512,512]{1,0:T(8,128)(2,1)} custom-call(bf16[64,512]{1,0:T(8,128)(2,1)} %bitcast.5, bf16[64,512]{1,0:T(8,128)(2,1)} %bitcast.6, s32[1,512]{1,0:T(1,128)} %bitcast.8, f32[8]{0:T(128)} %sink_ref.1, bf16[512,512]{1,0:T(8,128)(2,1)} %query_ref.1, bf16[512,2048]{1,0:T(8,128)(2,1)} %out_proj_ref.1, bf16[512,2048]{1,0:T(8,128)(2,1)} %residual_ref.1, ...), custom_call_target="tpu_custom_call" | custom-call | tf_op jit(solution)/shard_map/layer/pallas_call | solution.py:965
  143.6 1.9 %copy.16 = bf16[512,512]{1,0:T(8,128)(2,1)} copy(bf16[512,512]{1,0:T(8,128)(2,1)} %layer.1) | data formatting | bytes 1048576

commit v3 on v2

--- a/solution.py
+++ b/solution.py
@@ -156,18 +156,40 @@
 MIDDLE = (
     [("col", 1, 1, i) for i in PAIR]
     + [("far", 2, 0, 0)]
-    + [("col", 2, 1, i) for i in PAIR]
-    + [("row", 2, 0, i) for i in PAIR]
     + [(kind, 0, k, i) for i in PAIR for kind, k in (("col", 2), ("col", 3), ("row", 1))]
     + [("norm", 0, 0, 0)]
     + [("row", 1, 1, i) for i in PAIR]
     + [(kind, w, k, i) for i in PAIR for w, kind, k in ((1, "col", 2), (0, "row", 2), (1, "col", 3), (0, "row", 3))]
+    + [("col", 2, 1, i) for i in PAIR]
     + [("row", 1, k, i) for i in PAIR for k in (2, 3)]
 )
-UP_SERVE = ((2, [("row", 2, 1, 0)]), (4, [("row", 2, 1, 1)]))
+UP_SERVE = (
+    (0, [("row", 2, 0, i) for i in PAIR]),
+    (1, [("row", 2, 1, i) for i in PAIR]),
+    (2, [("col", 2, 2, 0)]),
+    (3, [("col", 2, 2, 1), ("col", 2, 3, 0)]),
+    (4, [("col", 2, 3, 1)]),
+)
+X_FIRST = ((0, 1), (1, 1))
+DOWN_ORDER = (
+    ("down", 0, 0),
+    ("down", 0, 1),
+    ("down", 1, 0),
+    ("down", 1, 1),
+    ("down", 2, 0),
+    ("down", 3, 0),
+    ("down", 2, 1),
+    ("cross", 2, 0),
+    ("down", 3, 1),
+    ("cross", 0, 0),
+    ("cross", 0, 1),
+    ("cross", 1, 0),
+    ("cross", 1, 1),
+    ("cross", 3, 0),
+    ("cross", 2, 1),
+    ("cross", 3, 1),
+)
 DOWN_SERVE = {
-    (2, 0): [("col", 2, 2, i) for i in PAIR],
-    (3, 0): [("col", 2, 3, i) for i in PAIR],
     (2, 1): [("row", 2, 2, i) for i in PAIR],
     (3, 1): [("row", 2, 3, i) for i in PAIR],
 }
@@ -218,6 +240,7 @@
     hidden,
     terms,
     terms_in,
+    from_mate,
     second,
     stats,
     plane_send,
@@ -242,6 +265,7 @@
     tail_recv,
     term_send,
     term_recv,
+    mate_recv,
     stat_send,
     stat_recv,
 ):
@@ -263,7 +287,6 @@
     home = low == core
     base = sp - 2 * low
     work = base + 2 * core
-    unit = 2 * x + low
     partner = base + 2 * (1 - low)
     sibling = 2 * x + 1 - core
     facing = 2 * (1 - x) + core
@@ -477,7 +500,6 @@
     near_sends(2)
     own_row(0)
     own_row(1)
-    own_row(2)
     settle = [
         pltpu.make_async_copy(own[w], slab(w, sp), local_sem.at[6 + w]) for w in range(3)
     ]
@@ -601,6 +623,7 @@
     lax.fori_loop(0, n_tp, attend_block, 0)
 
     serve(EARLY)
+    own_row(2)
     pair_copy(1, tp).wait_recv()
     facing_copy().wait_recv()
     first = mix_scale * rest[...].astype(F32) + parts[tp].astype(F32)
@@ -760,72 +783,122 @@
             total = total + tap * (shifted * mask_cols[lag, PAD : PAD + rows, :])
         return total
 
-    def up_block(c, carry):
+    def project(c, pair):
         at = pl.multiple_of(c * LANES, LANES)
         weights = jnp.concatenate(
             [gate_all[:, pl.ds(at, LANES)], value_all[:, pl.ds(at, LANES)]], axis=1
         )
         both = jnp.dot(normed[...], weights, preferred_element_type=F32)
         both = both.astype(BF16).astype(F32)
-        up_gate[...] = both[:, :LANES]
-        up_value[...] = both[:, LANES:]
-        gate = convolved(up_gate, taps_gate, at)
-        value = convolved(up_value, taps_value, at)
+        pair[0][...] = both[:, :LANES]
+        pair[1][...] = both[:, LANES:]
+
+    def activate(c, pair):
+        at = pl.multiple_of(c * LANES, LANES)
+        gate = convolved(pair[0], taps_gate, at)
+        value = convolved(pair[1], taps_value, at)
         inside = math.sqrt(2.0 / math.pi) * (gate + 0.044715 * (gate * gate * gate))
         hidden[:, pl.ds(at, LANES)] = (0.5 * gate * (1.0 + jnp.tanh(inside)) * value).astype(BF16)
+
+    even, odd = (up_gate.at[0], up_value.at[0]), (up_gate.at[1], up_value.at[1])
+    steps = ff // LANES
+    project(0, even)
+
+    def up_block(d, carry):
+        c = 2 * d
+        activate(c, even)
+        project(c + 1, odd)
+        activate(c + 1, odd)
+        project(c + 2, even)
         for at_step, events in UP_SERVE:
-            @pl.when(c == at_step)
+            @pl.when(d == at_step)
             def _():
                 serve(events)
 
         return carry
 
-    lax.fori_loop(0, ff // LANES, up_block, 0)
-
-    def term_copy(index, source):
-        owner = index // per
+    lax.fori_loop(0, (steps - 1) // 2, up_block, 0)
+    activate(steps - 1, even)
+
+    def term_copy(index, target, where, sem, device):
         return pltpu.make_async_remote_copy(
             src_ref=terms.at[index],
-            dst_ref=terms_in.at[source, lax.rem(index, per)],
+            dst_ref=target.at[where],
             send_sem=term_send.at[index],
-            recv_sem=term_recv.at[source, lax.rem(index, per)],
-            device_id=(work, owner),
-            device_id_type=MESH,
-        )
+            recv_sem=sem.at[where],
+            device_id=device,
+            device_id_type=MESH,
+        )
+
+    def to_owner(index, source, device):
+        return term_copy(index, terms_in, per * source + lax.rem(index, per), term_recv, device)
+
+    def to_mate(index, over_x):
+        device = (sp, facing) if over_x else (work, tp)
+        return term_copy(index, from_mate, lax.rem(index, 2 * per), mate_recv, device)
+
+    def slab_index(k, flip):
+        return 2 * zone(k) + (1 - y if flip else y)
 
     def down_block(k, flip):
-        index = 2 * zone(k) + (1 - y if flip else y)
-
+        index = slab_index(k, flip)
+        owner = index // per
+        crossing = owner // 2 != x
         serve(DOWN_SERVE.get((k, flip), ()))
         await_slab(2, k, flip)
         terms[index] = jnp.dot(
             hidden[...], down_all[index], preferred_element_type=F32
         ).astype(BF16)
 
-        mine = home & (index // per == tp)
-
-        @pl.when(mine)
-        def _():
-            terms_in[tp, lax.rem(index, per)] = terms[index]
-
-        @pl.when(jnp.logical_not(mine))
-        def _():
-            term_copy(index, unit).start()
-
-    for k, flip in ((0, 0), (0, 1), (1, 0), (1, 1), (2, 0), (3, 0), (2, 1), (3, 1)):
-        down_block(k, flip)
-
-    for source in range(n_tp):
-        @pl.when(jnp.logical_not(home & (tp == source)))
+        @pl.when(home & (owner == tp))
+        def _():
+            terms_in[lax.rem(index, per)] = terms[index]
+
+        @pl.when(home & (owner == sibling))
+        def _():
+            to_owner(index, 0, (sp, sibling)).start()
+
+        if (k, flip) in X_FIRST:
+            @pl.when(home & crossing)
+            def _():
+                to_owner(index, 2, (sp, owner)).start()
+        else:
+            @pl.when(jnp.logical_not(home | crossing))
+            def _():
+                to_owner(index, 1, (work, owner)).start()
+
+        @pl.when(jnp.logical_not(home) & crossing)
+        def _():
+            to_mate(index, (k, flip) in X_FIRST).start()
+
+    def cross_block(k, flip):
+        index = slab_index(k, flip)
+        owner = index // per
+
+        crossing = owner // 2 != x
+
+        over_x = (k, flip) in X_FIRST
+
+        @pl.when(jnp.logical_not(home | crossing) if over_x else home & crossing)
+        def _():
+            to_mate(index, over_x).wait_recv()
+            terms[index] = (
+                terms[index].astype(F32) + from_mate[lax.rem(index, 2 * per)].astype(F32)
+            ).astype(BF16)
+            if over_x:
+                to_owner(index, 1, (work, owner)).start()
+            else:
+                to_owner(index, 2, (sp, owner)).start()
+
+    for step, k, flip in DOWN_ORDER:
+        (down_block if step == "down" else cross_block)(k, flip)
+
+    for source in range(3):
+        @pl.when(jnp.logical_not(home) if source == 0 else tp >= 0)
         def _():
             for j in range(per):
-                pltpu.make_async_remote_copy(
-                    src_ref=terms_in.at[source, j],
-                    dst_ref=terms_in.at[source, j],
-                    send_sem=term_send.at[0],
-                    recv_sem=term_recv.at[source, j],
-                    device_id=(sp, sibling),
-                    device_id_type=MESH,
+                term_copy(
+                    0, terms_in, per * source + j, term_recv, (sp, sibling)
                 ).wait_recv()
 
     for i, peer in enumerate(peers):
@@ -835,8 +908,8 @@
     squares = jnp.zeros((rows, 1), F32)
     for j in range(per):
         total = mix_scale * norm_cols[:, j * cols : (j + 1) * cols].astype(F32)
-        for source in range(n_tp):
-            total = total + terms_in[source, j].astype(F32)
+        for source in range(3):
+            total = total + terms_in[per * source + j].astype(F32)
         second[:, j * cols : (j + 1) * cols] = total
         sums = sums + jnp.sum(total, axis=1, keepdims=True)
         squares = squares + jnp.sum(total * total, axis=1, keepdims=True)
@@ -916,7 +989,7 @@
     for index in range(n):
         @pl.when(jnp.logical_not(home & (tp == index // per)))
         def _():
-            term_copy(index, unit).wait_send()
+            to_mate(index, 0).wait_send()
 
     for peer in peers:
         stat_copy(peer, peer).wait_recv()
@@ -991,11 +1064,12 @@
             pltpu.VMEM((share, width), BF16),
             pltpu.VMEM((rows, width // n_tp), BF16),
             pltpu.VMEM((PAD + rows, width), BF16),
-            pltpu.VMEM((PAD + rows, LANES), F32),
-            pltpu.VMEM((PAD + rows, LANES), F32),
+            pltpu.VMEM((2, PAD + rows, LANES), F32),
+            pltpu.VMEM((2, PAD + rows, LANES), F32),
             pltpu.VMEM((rows, ff), BF16),
             pltpu.VMEM((n, rows, cols), BF16),
-            pltpu.VMEM((n_tp, per, rows, cols), BF16),
+            pltpu.VMEM((3 * per, rows, cols), BF16),
+            pltpu.VMEM((2 * per, rows, cols), BF16),
             pltpu.VMEM((rows, width // n_tp), F32),
             pltpu.VMEM((n_tp, 8, rows), F32),
             dma((3, 2, CHUNKS)),
@@ -1019,7 +1093,8 @@
             dma((n_tp,)),
             dma(()),
             dma((n,)),
-            dma((n_tp, per)),
+            dma((3 * per,)),
+            dma((2 * per,)),
             dma((n_tp,)),
             dma((n_tp,)),
         ],
@@ -1059,7 +1134,7 @@
         and key_rows.shape[1] == HD
         and query_rows.shape[1] % LANES == 0
         and depth % (16 * CHUNKS) == 0
-        and ff % LANES == 0
+        and ff % (2 * LANES) == LANES
         and ff % (16 * CHUNKS) == 0
         and cols % LANES == 0
         and share % cols == 0

time: 146 us -> 137 us (0.938)
  Pallas kernels: 144 us -> 135 us
    pallas_call x1, Pallas kernels: 144 us -> 135 us  [fused(): pl.pallas_call(functools.partial(layer_kernel, n, n_tp), out_shape=jax.Sh...]
where the time goes in v3:
time: 137 us
  Pallas kernels  135 us (99%)
  local copies, waits for them, and re-layouts  1.87 us (1%)
    pallas_call x1, Pallas kernels, fused(): pl.pallas_call(functools.partial(layer_kernel, n, n_tp), out_shape=jax.Sh...  135 us

profile of v3, /device:TPU:0, one launch (start us, length us, event | category | flops | bytes accessed | tf_op | source)
XLA Modules:
  0.0 136.6 jit_solution(8700539456092543267)
XLA Ops:
  0.0 134.7 %layer.1 = bf16[512,512]{1,0:T(8,128)(2,1)} custom-call(bf16[64,512]{1,0:T(8,128)(2,1)} %bitcast.5, bf16[64,512]{1,0:T(8,128)(2,1)} %bitcast.6, s32[1,512]{1,0:T(1,128)} %bitcast.8, f32[8]{0:T(128)} %sink_ref.1, bf16[512,512]{1,0:T(8,128)(2,1)} %query_ref.1, bf16[512,2048]{1,0:T(8,128)(2,1)} %out_proj_ref.1, bf16[512,2048]{1,0:T(8,128)(2,1)} %residual_ref.1, ...), custom_call_target="tpu_custom_call" | custom-call | tf_op jit(solution)/shard_map/layer/pallas_call | solution.py:1038
  134.8 1.9 %copy.16 = bf16[512,512]{1,0:T(8,128)(2,1)} copy(bf16[512,512]{1,0:T(8,128)(2,1)} %layer.1) | data formatting | bytes 1048576

commit v4 on v3

--- a/solution.py
+++ b/solution.py
@@ -496,6 +496,7 @@
         copy.start()
     near_sends(0)
     far_sends(0, inner | home)
+    far_sends(1, home & jnp.logical_not(inner))
     near_sends(1)
     near_sends(2)
     own_row(0)
@@ -701,7 +702,6 @@
         def _():
             norm_copy(i, device, tp).start()
 
-    far_sends(1, home & jnp.logical_not(inner))
     far_sends(2, home & jnp.logical_not(inner))
     for i, peer in enumerate(peers):
         cols_copy(i, peer, tp).start()

time: 137 us -> 137 us (level)
  no operation moved by 1% of the time
where the time goes in v4:
time: 137 us
  Pallas kernels  135 us (99%)
  local copies, waits for them, and re-layouts  1.87 us (1%)
    pallas_call x1, Pallas kernels, fused(): pl.pallas_call(functools.partial(layer_kernel, n, n_tp), out_shape=jax.Sh...  135 us

profile of v4, /device:TPU:0, one launch (start us, length us, event | category | flops | bytes accessed | tf_op | source)
XLA Modules:
  0.0 136.6 jit_solution(4623643752072167219)
XLA Ops:
  0.0 134.7 %layer.1 = bf16[512,512]{1,0:T(8,128)(2,1)} custom-call(bf16[64,512]{1,0:T(8,128)(2,1)} %bitcast.5, bf16[64,512]{1,0:T(8,128)(2,1)} %bitcast.6, s32[1,512]{1,0:T(1,128)} %bitcast.8, f32[8]{0:T(128)} %sink_ref.1, bf16[512,512]{1,0:T(8,128)(2,1)} %query_ref.1, bf16[512,2048]{1,0:T(8,128)(2,1)} %out_proj_ref.1, bf16[512,2048]{1,0:T(8,128)(2,1)} %residual_ref.1, ...), custom_call_target="tpu_custom_call" | custom-call | tf_op jit(solution)/shard_map/layer/pallas_call | solution.py:1038
  134.7 1.9 %copy.16 = bf16[512,512]{1,0:T(8,128)(2,1)} copy(bf16[512,512]{1,0:T(8,128)(2,1)} %layer.1) | data formatting | bytes 1048576
